TPU v7x, 256 devices: a 4x2x16 block of a 4x16x16 slice. The times are simulated.
256 devices in a mesh: grp: 2 (over y), fs: 16 (over z), tp: 8 (over x, core).
Axes of the slice: x: 4, y: 2, z: 16, core: 2. Of those that a mesh axis runs over, the one named last changes fastest.
The devices are a block of a 4x16x16 slice.
Arguments:
- incoming_representations: bfloat16 [20480, 2048], P(('grp', 'fs', 'tp')), parts along dimension 0, may hold values from -6 to 6
- perceptron_switch_coefficients: bfloat16 [2048, 5120], P('fs', 'tp'), may hold values from -0.125 to 0.125
- perceptron_expand_coefficients: bfloat16 [2048, 5120], P('fs', 'tp'), may hold values from -0.125 to 0.125
- perceptron_contract_coefficients: bfloat16 [5120, 2048], P('tp', 'fs'), may hold values from -0.5 to 0.5
- probe_coefficients: bfloat16 [2048, 512], P('fs', 'tp'), may hold values from -0.125 to 0.125
- address_coefficients: bfloat16 [2048, 512], P('fs', 'tp'), may hold values from -0.125 to 0.125
- payload_coefficients: bfloat16 [2048, 1024], P('fs', 'tp'), may hold values from -0.125 to 0.125
- emit_switch_coefficients: bfloat16 [2048, 1024], P('fs', 'tp'), may hold values from -0.125 to 0.125
- forgetting_shrink_coefficients: bfloat16 [2048, 32], replicated, may hold values from -0.125 to 0.125
- forgetting_expand_coefficients: bfloat16 [32, 512], P(None, 'tp'), may hold values from -3 to 3
- forgetting_sigmoid_intercept: float32 [512], P('tp'), may hold values from -1 to 9
- extra_forgetting_logits: float32 [20480, 512], P(('grp', 'fs'), 'tp'), parts along dimension 0, may hold values from -0.7 to 0
- subspace_rescaling_amplitude: float32 [128], replicated, may hold values from 0.1 to 1.9
- recurrence_emit_coefficients: bfloat16 [1024, 2048], P('tp', 'fs'), may hold values from -0.5 to 0.5
Outputs:
- layer_out: bfloat16 [20480, 2048], P(('grp', 'fs', 'tp')), parts along dimension 0
There are 2 independent parts, one for each index of `grp`. A program takes and returns all parts, laid end to end along the dimension named above; an argument that names none is the same for every part. Nothing has to cross between parts.
All inputs are finite; a program needn't handle non-finite values.
Results may differ from a plain program's by a relative error of at most 0.035.
Values may be sent and summed in bfloat16 or wider, within the bound.
A program may use at most 64 MiB of HBM per device.

v0:
```python
import jax
import jax.numpy as jnp
from jax import lax
from jax.sharding import PartitionSpec as P

DK = 64
DV = 128
BLOCK = 64
SEQUENCE_LENGTH = 320


residual_gain = 1.681792830507429
forgetting_steepness_multiplier = 16.0
epsilon = 1e-06


def in_order(tiles, dim):
    tiles = jnp.moveaxis(tiles, 0, dim)
    dims = tiles.shape
    return tiles.reshape(*dims[:dim], dims[dim] * dims[dim + 1], *dims[dim + 2 :])


def sent_to_all(x, axis):
    copies = jnp.broadcast_to(x, (lax.axis_size(axis), *x.shape))
    return lax.all_to_all(copies, axis, split_axis=0, concat_axis=0, tiled=True)


def collect(x, axis, dim):
    return in_order(sent_to_all(x, axis), dim)


def cut_along(x, dim, peers):
    dims = x.shape
    tiles = x.reshape(*dims[:dim], peers, dims[dim] // peers, *dims[dim + 1 :])
    return jnp.moveaxis(tiles, dim, 0)


def sent_and_summed(x, axis, dim):
    tiles = cut_along(x, dim, lax.axis_size(axis))
    arrived = lax.all_to_all(tiles, axis, split_axis=0, concat_axis=0, tiled=True)
    return arrived.astype(jnp.float32).sum(axis=0)


def in_one_piece(arrays, axis, dim, along):
    both = jnp.concatenate(arrays, axis=along)
    whole, at, done = (lax.all_gather(both, axis, axis=dim, tiled=True), 0, [])
    for a in arrays:
        done.append(lax.slice_in_dim(whole, at, at + a.shape[along], axis=along))
        at += a.shape[along]
    return tuple(done)


def post_norm(residual, branch):
    summed = residual_gain * residual.astype(jnp.float32) + branch
    average = jnp.mean(summed, axis=-1, keepdims=True)
    centred = summed - average
    variance = jnp.mean(centred * centred, axis=-1, keepdims=True)
    return (centred * lax.rsqrt(variance + epsilon)).astype(jnp.bfloat16)


def gather_group(stored):
    return collect(stored, "tp", 0)


def return_rows(hidden, weight_full):
    return sent_and_summed(
        jnp.dot(hidden, weight_full, preferred_element_type=jnp.float32).astype(jnp.bfloat16),
        "tp",
        0,
    )


def blockwise_mixing(queries, key_rows, values, forgetting_euler_power):
    token_count = queries.shape[0]
    head_count = queries.shape[1] // DK
    seq_count = token_count // SEQUENCE_LENGTH
    block_count = SEQUENCE_LENGTH // BLOCK

    def to_blocks(source, channels):
        shaped = source.astype(jnp.float32).reshape(
            seq_count, block_count, BLOCK, head_count, channels
        )
        return shaped.transpose(0, 3, 1, 2, 4)

    query_blk = to_blocks(queries, DK)
    key_blk = to_blocks(key_rows, DK)
    value_blk = to_blocks(values, DV)
    decay_blk = to_blocks(forgetting_euler_power, DK)
    inclusive = jnp.cumsum(decay_blk, axis=3)
    exclusive = inclusive - decay_blk
    block_end = inclusive[:, :, :, BLOCK - 1 :, :]
    token_positions = jnp.arange(BLOCK)
    lower_mask = (token_positions[:, None] >= token_positions[None, :])[:, :, None]
    flat_lead = seq_count * head_count * block_count

    def flatten(source):
        return source.reshape((flat_lead, BLOCK, source.shape[-1]))

    def within_block(inputs):
        query_one, key_one, value_one, incl_one, excl_one = inputs
        spread = jnp.where(
            lower_mask,
            incl_one[:, None, :] - incl_one[None, :, :],
            excl_one[None, :, :] - excl_one[:, None, :],
        )
        scores = jnp.sum(query_one[:, None, :] * key_one[None, :, :] * jnp.exp(spread), axis=-1)
        return jnp.dot(scores, value_one)

    local_out = lax.map(
        within_block,
        (
            flatten(query_blk),
            flatten(key_blk),
            flatten(value_blk),
            flatten(inclusive),
            flatten(exclusive),
        ),
    )
    local_out = local_out.reshape(value_blk.shape)
    forward_keys = key_blk * jnp.exp(block_end - inclusive)
    backward_keys = key_blk * jnp.exp(exclusive)
    forward_sums = jnp.einsum("shnld,shnlv->nshdv", forward_keys, value_blk)
    backward_sums = jnp.einsum("shnld,shnlv->nshdv", backward_keys, value_blk)
    through = jnp.moveaxis(jnp.exp(block_end[:, :, :, 0, :]), 2, 0)

    def advance(carried, inputs):
        block_sum, segment_passing_across = inputs
        return (segment_passing_across[..., None] * carried + block_sum, carried)

    start_state = jnp.zeros(forward_sums.shape[1:], jnp.float32)
    _, before = lax.scan(advance, start_state, (forward_sums, through))
    _, after = lax.scan(advance, start_state, (backward_sums, through), reverse=True)
    carried_out = jnp.einsum("shnld,nshdv->shnlv", query_blk * jnp.exp(inclusive), before)
    carried_out = carried_out + jnp.einsum(
        "shnld,nshdv->shnlv", query_blk * jnp.exp(block_end - exclusive), after
    )
    combined = local_out + carried_out
    return combined.transpose(0, 2, 3, 1, 4).reshape(token_count, head_count, DV)


def per_device(
    incoming_representations,
    perceptron_switch_coefficients,
    perceptron_expand_coefficients,
    perceptron_contract_coefficients,
    probe_coefficients,
    address_coefficients,
    payload_coefficients,
    emit_switch_coefficients,
    forgetting_shrink_coefficients,
    forgetting_expand_coefficients,
    forgetting_sigmoid_intercept,
    extra_forgetting_logits,
    subspace_rescaling_amplitude,
    recurrence_emit_coefficients,
):
    gate_full, up_full = in_one_piece(
        (perceptron_switch_coefficients, perceptron_expand_coefficients), "fs", 0, 1
    )
    down_kept = lax.all_gather(perceptron_contract_coefficients, "fs", axis=1, tiled=True)

    def expand(gathered):
        return (
            jnp.dot(gathered, gate_full, preferred_element_type=jnp.float32),
            jnp.dot(gathered, up_full, preferred_element_type=jnp.float32),
        )

    def channel_half(stored):
        gathered = gather_group(stored)
        gate_sum, up_sum = expand(gathered)
        hidden = (jax.nn.silu(gate_sum) * up_sum).astype(jnp.bfloat16)
        return post_norm(stored, 0.5 * return_rows(hidden, down_kept))

    opening_perceptron_result = channel_half(incoming_representations)
    gathered = gather_group(opening_perceptron_result)
    pieces = in_one_piece(
        (probe_coefficients, address_coefficients, payload_coefficients, emit_switch_coefficients),
        "fs",
        0,
        1,
    )
    projected = tuple(
        (jnp.dot(gathered, piece_one, preferred_element_type=jnp.float32) for piece_one in pieces)
    )
    queries, key_rows, values, outgate = [summed.astype(jnp.bfloat16) for summed in projected]
    compact_inner_dimensionality = jnp.dot(
        gathered, forgetting_shrink_coefficients, preferred_element_type=jnp.float32
    ).astype(jnp.bfloat16)
    forgetting_euler_power = (
        jax.nn.log_sigmoid(
            jnp.dot(
                compact_inner_dimensionality,
                forgetting_expand_coefficients,
                preferred_element_type=jnp.float32,
            )
            + forgetting_sigmoid_intercept
        )
        / forgetting_steepness_multiplier
        + extra_forgetting_logits
    )
    mixed_heads = blockwise_mixing(queries, key_rows, values, forgetting_euler_power)
    scaled = (
        mixed_heads
        * lax.rsqrt(jnp.mean(mixed_heads * mixed_heads, axis=-1, keepdims=True) + epsilon)
        * subspace_rescaling_amplitude
    )
    opener = jax.nn.silu(outgate.astype(jnp.float32)).reshape(mixed_heads.shape)
    gated = (scaled * opener).reshape(mixed_heads.shape[0], -1).astype(jnp.bfloat16)
    out_full = collect(recurrence_emit_coefficients, "fs", 1)
    context_blend_result = post_norm(opening_perceptron_result, return_rows(gated, out_full))
    return channel_half(context_blend_result)


def solution(mesh):
    return jax.shard_map(
        per_device,
        mesh=mesh,
        in_specs=(
            P(("grp", "fs", "tp"), None),
            P("fs", "tp"),
            P("fs", "tp"),
            P("tp", "fs"),
            P("fs", "tp"),
            P("fs", "tp"),
            P("fs", "tp"),
            P("fs", "tp"),
            P(),
            P(None, "tp"),
            P("tp"),
            P(("grp", "fs"), "tp"),
            P(),
            P("tp", "fs"),
        ),
        out_specs=P(("grp", "fs", "tp"), None),
        check_vma=False,
    )
```

profile of v0, /device:TPU:33, one launch (start us, length us, event | category | flops | bytes accessed | tf_op | source)
XLA Modules:
  0.0 500.8 jit_solution(16295634164969662825)
XLA Ops:
  10.5 54.8 %all_to_all.35 = bf16[8,80,2048]{2,1,0:T(8,128)(2,1)S(1)} all-to-all(bf16[8,80,2048]{2,1,0:T(8,128)(2,1)S(1)} %broadcast_in_dim.65), channel_id=1, replica_groups=mesh['grp'=2,'fs'=16,'tp'=8] {'tp'}, dimensions={0} | all-to-all | bytes 5242880 | tf_op jit(solution)/shard_map/all_to_all | solution.py:25
  65.3 29.9 %all-gather.4.cloned.1.call-done = bf16[2048,1280]{1,0:T(8,128)(2,1)} async-done(((bf16[128,1280]{1,0:T(8,128)(2,1)}), bf16[2048,1280]{1,0:T(8,128)(2,1)}) %all-gather.4.cloned.1.call-update) | async-done | bytes 5242896 | tf_op jit(solution)/shard_map/all_gather | solution.py:46
  95.1 5.1 %fusion.15 = f32[640,640]{1,0:T(8,128)} fusion(bf16[640,2048]{1,0:T(8,128)(2,1)S(1)} %bitcast.213, bf16[2048,1280]{1,0:T(8,128)(2,1)} %all-gather.4.cloned.1.call-done), kind=kOutput, calls=%fused_computation.35 | convolution fusion | flops 1677721600 | bytes 6881280 | tf_op jit(solution)/shard_map/dot_general | solution.py:164
  100.3 70.1 %all-gather.6.cloned.1.call-done = bf16[640,2048]{1,0:T(8,128)(2,1)} async-done(((bf16[640,128]{1,0:T(8,128)(2,1)}), bf16[640,2048]{1,0:T(8,128)(2,1)}) %all-gather.6.cloned.1.call-update) | async-done | bytes 2621456 | tf_op jit(solution)/shard_map/all_gather | solution.py:160
  170.3 12.9 %convolution_convert_fusion.1 = bf16[640,2048]{1,0:T(8,128)(2,1)} fusion(bf16[640,2048]{1,0:T(8,128)(2,1)} %all-gather.6.cloned.1.call-done, f32[640,640]{1,0:T(8,128)} %fusion.15, bf16[640,2048]{1,0:T(8,128)(2,1)S(1)} %bitcast.214, bf16[2048,1280]{1,0:T(8,128)(2,1)} %all-gather.4.cloned.1.call-done), kind=kOutput, calls=%fused_computation.27 | convolution fusion | flops 3359211520 | bytes 12124160 | tf_op jit(solution)/shard_map/dot_general | solution.py:67
  183.2 16.1 %all-to-all-start.1 = ((bf16[8,80,2048]{2,1,0:T(8,128)(2,1)}), bf16[8,80,2048]{2,1,0:T(8,128)(2,1)S(1)}, u32[]{:S(2)}, u32[]{:S(2)}) async-start(bf16[8,80,2048]{2,1,0:T(8,128)(2,1)} %bitcast.212), calls=%async_computation.1 | async-start | bytes 5242880 | tf_op jit(solution)/shard_map/all_to_all | solution.py:40
  200.4 30.8 %all-to-all-done.1 = bf16[8,80,2048]{2,1,0:T(8,128)(2,1)S(1)} async-done(((bf16[8,80,2048]{2,1,0:T(8,128)(2,1)}), bf16[8,80,2048]{2,1,0:T(8,128)(2,1)S(1)}, u32[]{:S(2)}, u32[]{:S(2)}) %all-to-all-start.1) | async-done | bytes 2621472 | tf_op jit(solution)/shard_map/all_to_all | solution.py:40
  234.2 4.6 all-to-all-start.2
  239.0 31.8 %all-to-all-done.2 = bf16[8,80,2048]{2,1,0:T(8,128)(2,1)S(1)} async-done(((bf16[8,80,2048]{2,1,0:T(8,128)(2,1)}), bf16[8,80,2048]{2,1,0:T(8,128)(2,1)S(1)}, u32[]{:S(2)}, u32[]{:S(2)}) %all-to-all-start.2) | async-done | bytes 2621472 | tf_op jit(solution)/shard_map/all_to_all | solution.py:25
  271.7 7.1 %all-to-all-start.3 = ((bf16[16,128,128]{1,2,0:T(8,128)(2,1)}), bf16[16,128,128]{1,2,0:T(8,128)(2,1)}, u32[]{:S(2)}, u32[]{:S(2)}) async-start(bf16[16,128,128]{1,2,0:T(8,128)(2,1)} %broadcast_in_dim.69), calls=%async_computation.3 | async-start | bytes 1048576 | tf_op jit(solution)/shard_map/all_to_all | solution.py:25
  278.9 2.0 fusion.29
  281.8 2.0 fusion.28
  290.3 2.5 convolution_convert_fusion.4
  292.9 44.2 %while.41 = (s32[]{:T(128)}, f32[10,64,128]{2,1,0:T(8,128)}, f32[10,64,64]{2,1,0:T(8,128)}, f32[10,64,64]{2,1,0:T(8,128)}, f32[10,64,64]{2,1,0:T(8,128)S(1)}, /*...) while((s32[]{:T(128)}, f32[10,64,128]{2,1,0:T(8,128)}, ...), condition=%wide.region_6.7_spmd.clone, body=%wide.region_4.6_spmd.clone.sunk | while | flops 2621442 | bytes 271461 | solution.py:109
  340.9 1.9 convolution_bitcast_fusion.1
  343.5 7.9 %while.43 = (s32[]{:T(128)}, f32[2,1,64,128]{3,2,1,0:T(8,128)S(1)}, bf16[5,2,1,64,128]{4,3,1,2,0:T(8,128)(2,1)}, f32[5,2,1,64]{3,1,2,0:T(2,128)S(1)}, f32[5,2,1,...) while((s32[]{:T(128)}, f32[2,1,64,128]{3,2,1,0:T(8,128)S(1)}, ...), condition=%wide.region_10.11_spmd.clone, body=%wide.region_9.10_spmd.clone.sunk | while | flops 65540 | bytes 296576 | solution.py:132
  352.1 7.8 %while.42 = (s32[]{:T(128)}, f32[2,1,64,128]{3,2,1,0:T(8,128)S(1)}, bf16[5,2,1,64,128]{4,3,1,2,0:T(8,128)(2,1)}, f32[5,2,1,64]{3,1,2,0:T(2,128)S(1)}, f32[5,2,1,64,128]{4,3,1,2,0:T(8,128)}, /*index=5*/s32[]{:T(128)}, s32[]{:T(128)}) while((s32[]{:T(128)}, f32[2,1,64,128]{3,2,1,0:T(8,128)S(1)}, ...), condition=%wide.region_8.9_spmd.clone, body=%wide.region_7.8_spmd.clone.sunk | while | flops 65539 | bytes 296556 | solution.py:131
  361.1 2.2 multiply_reduce_fusion.4
  363.4 2.0 fusion.42
  367.3 35.6 %all_to_all.36 = bf16[8,80,2048]{2,1,0:T(8,128)(2,1)S(1)} all-to-all(bf16[8,80,2048]{2,1,0:T(8,128)(2,1)S(1)} %bitcast.200), channel_id=1, replica_groups=mesh['grp'=2,'fs'=16,'tp'=8] {'tp'}, dimensions={0} | all-to-all | bytes 5242880 | tf_op jit(solution)/shard_map/all_to_all | solution.py:40
  404.2 35.5 %all_to_all.37 = bf16[8,80,2048]{2,1,0:T(8,128)(2,1)S(1)} all-to-all(bf16[8,80,2048]{2,1,0:T(8,128)(2,1)S(1)} %broadcast_in_dim.70), channel_id=1, replica_groups=mesh['grp'=2,'fs'=16,'tp'=8] {'tp'}, dimensions={0} | all-to-all | bytes 5242880 | tf_op jit(solution)/shard_map/all_to_all | solution.py:25
  439.8 3.4 fusion.13
  443.1 12.9 %convolution_convert_fusion = bf16[640,2048]{1,0:T(8,128)(2,1)} fusion(bf16[640,2048]{1,0:T(8,128)(2,1)} %all-gather.6.cloned.1.call-done, f32[640,640]{0,1:T(8,128)} %fusion.13, bf16[640,2048]{1,0:T(8,128)(2,1)S(1)} %bitcast.216, bf16[2048,1280]{1,0:T(8,128)(2,1)} %all-gather.4.cloned.1.call-done), kind=kOutput, calls=%fused_computation.26 | convolution fusion | flops 3359211520 | bytes 12124160 | tf_op jit(solution)/shard_map/dot_general | solution.py:67
  456.0 36.4 %all_to_all.38 = bf16[8,80,2048]{2,1,0:T(8,128)(2,1)S(1)} all-to-all(bf16[8,80,2048]{2,1,0:T(8,128)(2,1)} %bitcast.217), channel_id=1, replica_groups=mesh['grp'=2,'fs'=16,'tp'=8] {'tp'}, dimensions={0} | all-to-all | bytes 5242880 | tf_op jit(solution)/shard_map/all_to_all | solution.py:40
  (163 shorter events, 87.7 us)
Async XLA Ops:
  6.5 278.2 %copy-start = (bf16[2048,32]{0,1:T(8,128)(2,1)S(1)}, bf16[2048,32]{0,1:T(8,128)(2,1)}, u32[]{:S(2)}) copy-start(bf16[2048,32]{0,1:T(8,128)(2,1)} %param.28) | copy-start | bytes 393220
  6.6 88.6 %all-gather.4.cloned.1.call-start = ((), (), s32[]{:S(2)}) async-start(), calls=%async_computation.7 | async-start | bytes 5570560 | tf_op jit(solution)/shard_map/all_gather | solution.py:46
  8.4 161.9 %all-gather.6.cloned.1.call-start = ((), (), s32[]{:S(2)}) async-start(), calls=%async_computation.8 | async-start | bytes 2785280 | tf_op jit(solution)/shard_map/all_gather | solution.py:160
  183.2 16.2 %copy-start.6 = (bf16[128,64]{0,1:T(8,128)(2,1)S(1)}, bf16[128,64]{0,1:T(8,128)(2,1)}, u32[]{:S(2)}) copy-start(bf16[128,64]{0,1:T(8,128)(2,1)} %param.25) | copy-start | bytes 49156
  183.2 16.3 %copy-start.7 = (bf16[128,64]{0,1:T(8,128)(2,1)S(1)}, bf16[128,64]{0,1:T(8,128)(2,1)}, u32[]{:S(2)}) copy-start(bf16[128,64]{0,1:T(8,128)(2,1)} %param.24) | copy-start | bytes 49156
  183.2 16.4 %copy-start.3 = (bf16[128,128]{1,0:T(8,128)(2,1)S(1)}, bf16[128,128]{1,0:T(8,128)(2,1)}, u32[]{:S(2)}) copy-start(bf16[128,128]{1,0:T(8,128)(2,1)} %param.27) | copy-start | bytes 98308
  183.2 16.4 %copy-start.4 = (bf16[128,128]{1,0:T(8,128)(2,1)S(1)}, bf16[128,128]{1,0:T(8,128)(2,1)}, u32[]{:S(2)}) copy-start(bf16[128,128]{1,0:T(8,128)(2,1)} %param.26) | copy-start | bytes 98308
  183.2 48.0 %all-to-all-start.1 = ((bf16[8,80,2048]{2,1,0:T(8,128)(2,1)}), bf16[8,80,2048]{2,1,0:T(8,128)(2,1)S(1)}, u32[]{:S(2)}, u32[]{:S(2)}) async-start(bf16[8,80,2048]{2,1,0:T(8,128)(2,1)} %bitcast.212), calls=%async_computation.1 | async-start | bytes 5242880 | tf_op jit(solution)/shard_map/all_to_all | solution.py:40
  199.3 32.3 %copy-start.1 = (bf16[80,2048]{1,0:T(8,128)(2,1)S(1)}, bf16[80,2048]{1,0:T(8,128)(2,1)}, u32[]{:S(2)}) copy-start(bf16[80,2048]{1,0:T(8,128)(2,1)} %param.20) | copy-start | bytes 983044
  199.3 79.5 %all-gather.8.cloned.1.call-start = ((), (), s32[]{:S(2)}) async-start(), calls=%async_computation.9 | async-start | bytes 1671168 | tf_op jit(solution)/shard_map/all_gather | solution.py:46
  234.2 4.7 copy-start.5
  234.2 36.6 %all-to-all-start.2 = ((bf16[8,80,2048]{2,1,0:T(8,128)(2,1)}), bf16[8,80,2048]{2,1,0:T(8,128)(2,1)S(1)}, u32[]{:S(2)}, u32[]{:S(2)}) async-start(bf16[8,80,2048]{2,1,0:T(8,128)(2,1)} %broadcast_in_dim.67), calls=%async_computation.2 | async-start | bytes 5242880 | tf_op jit(solution)/shard_map/all_to_all | solution.py:25
  271.7 93.7 %all-to-all-start.3 = ((bf16[16,128,128]{1,2,0:T(8,128)(2,1)}), bf16[16,128,128]{1,2,0:T(8,128)(2,1)}, u32[]{:S(2)}, u32[]{:S(2)}) async-start(bf16[16,128,128]{1,2,0:T(8,128)(2,1)} %broadcast_in_dim.69), calls=%async_computation.3 | async-start | bytes 1048576 | tf_op jit(solution)/shard_map/all_to_all | solution.py:25
  280.8 3.9 copy-start.2
  280.8 3.9 copy-start.8
  280.8 3.9 copy-start.9
  351.4 12.0 %copy-start.10 = (f32[128]{0:T(128)S(1)}, f32[128]{0:T(128)}, u32[]{:S(2)}) copy-start(f32[128]{0:T(128)} %param.32) | copy-start | bytes 1540
  403.3 36.5 %slice-start = ((s8[5242880]{0:T(1024)(128)(4,1)}), s8[4194304]{0:T(1024)(128)(4,1)S(1)}, s32[]{:S(2)}) async-start(s8[5242880]{0:T(1024)(128)(4,1)} %bitcast.225), calls=%async_computation.10 | async-start | bytes 8388608
  403.9 35.8 %slice-start.1 = ((s8[5242880]{0:T(1024)(128)(4,1)}), s8[1048576]{0:T(1024)(128)(4,1)S(1)}, s32[]{:S(2)}) async-start(s8[5242880]{0:T(1024)(128)(4,1)} %bitcast.225), calls=%async_computation.11 | async-start | bytes 2097152
Sparse Core Ops, SparseCore 0:
  9.1 85.9 all-gather.3
  96.9 73.4 all-gather.5
  201.9 56.6 all-gather.7
where the time goes:
time: 504 us; the launch traced here: 501 us
  waiting for transfers between devices  163 us (32%)
  blocking collectives  162 us (32%)
  matrix products  67.5 us (13%)
  other arithmetic  40.3 us (8%)
  starting transfers between devices  28 us (6%)
  local copies, waits for them, and re-layouts  25.8 us (5%)
  between operations  13.4 us (3%)
    all_to_all x2, blocking collectives, sent_to_all(): return lax.all_to_all(copies, axis, split_axis=0, concat_axis=0, tiled=True)  90.3 us
    all_to_all x2, blocking collectives, sent_and_summed(): lax.all_to_all(tiles, axis, split_axis=0, concat_axis=0, tiled=True)  72 us
    all_gather x1, waiting for transfers between devices, per_device(): lax.all_gather(perceptron_contract_coefficients, 'fs', axis=1, tiled=True)  70.1 us
    all_to_all x2, waiting for transfers between devices, sent_to_all(): return lax.all_to_all(copies, axis, split_axis=0, concat_axis=0, tiled=True)  31.8 us
    all_to_all x1, waiting for transfers between devices, sent_and_summed(): lax.all_to_all(tiles, axis, split_axis=0, concat_axis=0, tiled=True)  30.8 us
    all_gather x2, waiting for transfers between devices, in_one_piece(): whole, at, done = (lax.all_gather(both, axis, axis=dim, tiled=True), 0, [])  29.9 us
    dot_general x3, matrix products, return_rows(): jnp.dot(hidden, weight_full, preferred_element_type=jnp.float32)  27.6 us
    all_to_all x1, starting transfers between devices, sent_and_summed(): lax.all_to_all(tiles, axis, split_axis=0, concat_axis=0, tiled=True)  16.1 us
  transfers between devices with their start and end apart: 6, of which 4 were waited for; matrix products, arithmetic and copies ran while one was open for 19% of the time, Pallas kernels for 0%

commit v1 on v0

v1 whole, which is shorter than its diff:
```python
import functools

import jax
import jax.numpy as jnp
from jax import lax
from jax.experimental import pallas as pl
from jax.experimental.pallas import tpu as pltpu
from jax.sharding import PartitionSpec as P

MESH = pl.DeviceIdType.MESH
DK = 64
DV = 128
SEQ = 320
PAD = 384
GAIN = 1.681792830507429
STEEP = 16.0
EPS = 1e-06
CHUNKS = 2
OFFSETS = (0, 3, 6, 6)
RIGHT, LEFT = 0, 1
A, B = 0, 1
f32, bf16 = jnp.float32, jnp.bfloat16


def mo(v, m):
    return pl.multiple_of(v, m)


def dot(a, b):
    return jnp.dot(a, b, preferred_element_type=f32)


def dot_t(a, b):
    return lax.dot_general(a, b, (((1,), (1,)), ((), ())), preferred_element_type=f32)


def kernel(
    n,
    x_in, wsw, wex, wct, wq, wk, wv, wg, wls, wle, bias, extra, gain, wo,
    out,
    gu, dn, qb, ob, xg, hb, pp, rp, sm, st, rt, br,
    qk, vb, og, lg, mm, wle2, bias2, extra2, gt,
    z_recv, c_recv, z_send, ag_recv, ag_send, rs_recv, rs_send, loc,
):
    T, D = x_in.shape
    K = wsw.shape[0]
    F = wsw.shape[1]
    H = n // 2
    zi = lax.axis_index("fs")
    gi = lax.axis_index("grp")
    ti = lax.axis_index("tp")
    par = lax.rem(gi, 2)
    ci = lax.rem(ti, 2)
    xi = lax.div(ti, 2)
    oc = 1 - ci
    x1 = lax.rem(xi + 1, 4)
    x2 = lax.rem(xi + 2, 4)
    x3 = lax.rem(xi + 3, 4)
    z_right = {"fs": lax.rem(zi + 1, n)}
    z_left = {"fs": lax.rem(zi + n - 1, n)}
    y_dev = {"grp": gi + 1 - 2 * par}
    x_right = {"tp": x1 * 2 + ci}
    x_left = {"tp": x3 * 2 + ci}
    mate = {"tp": xi * 2 + oc}
    z_dev = (z_right, z_left)

    def remote(src, dst, s, r, dev):
        return pltpu.make_async_remote_copy(
            src_ref=src, dst_ref=dst, send_sem=s, recv_sem=r, device_id=dev, device_id_type=MESH
        )

    locals_ = []
    own = pl.ds(mo(zi * K, K), K)
    for j in range(F // 128):
        col = slice(j * 128, j * 128 + 128)
        locals_.append((wsw.at[:, col], gu.at[own, pl.ds(j * 256, 128)]))
        locals_.append((wex.at[:, col], gu.at[own, pl.ds(j * 256 + 128, 128)]))
    locals_.append((x_in, xg.at[0, pl.ds(mo((ci * 4 + xi) * T, 16), T)]))
    locals_.append((wct, dn.at[:, own]))
    locals_.append((wv, qb.at[own, pl.ds(128, 128)]))
    locals_.append((wg, qb.at[own, pl.ds(256, 128)]))
    locals_.append((wo, ob.at[:, own]))
    locals_ = [pltpu.make_async_copy(s, d, loc.at[i]) for i, (s, d) in enumerate(locals_)]
    for c in locals_:
        c.start()
    qb[own, 0:64] = wq[...]
    qb[own, 64:128] = wk[...]

    barrier = pltpu.get_barrier_semaphore()
    for dev in (z_right, z_left, y_dev, x_right, x_left, mate):
        pl.semaphore_signal(barrier, inc=1, device_id=dev, device_id_type=MESH)
    pl.semaphore_wait(barrier, 6)

    def rows_of(o):
        return pl.ds(mo(o * K, K), K)

    def gu_at(o, ch):
        return gu.at[rows_of(o), pl.ds(mo(par * 896, 128), 384) if ch == A else pl.ds(384, 512)]

    def dn_at(o, ch):
        return dn.at[pl.ds(mo(par * 432, 16), 208) if ch == A else pl.ds(208, 224), rows_of(o)]

    def qb_at(o, ch):
        return qb.at[rows_of(o), pl.ds(mo(par * 256, 128), 128) if ch == A else pl.ds(128, 128)]

    def ob_at(o, ch):
        return ob.at[pl.ds(mo(par * 80, 16), 48) if ch == A else pl.ds(48, 32), rows_of(o)]

    at = (gu_at, dn_at, qb_at, ob_at)
    R = (n - 1) * K
    whole = (
        (gu.at[0:R, 0:384], gu.at[0:R, 384:896]),
        (dn.at[0:208, 0:R], dn.at[208:432, 0:R]),
        (qb.at[0:R, 0:128], qb.at[0:R, 128:256]),
        (ob.at[0:48, 0:R], ob.at[48:80, 0:R]),
    )

    def steps_of(ch, d):
        return H if (ch == A) == (d == RIGHT) else H - 1

    def origin(d, back):
        return lax.rem(zi + n - back, n) if d == RIGHT else lax.rem(zi + back, n)

    def z_copy(m, ch, d, s, o):
        ref = at[m](o, ch)
        return remote(ref, ref, z_send.at[m, ch], z_recv.at[m, d, ch, s - 1], z_dev[d])

    def tick(t):
        for m in range(4):
            s = t - OFFSETS[m]
            if s < 1 or s > H + 1:
                continue
            for ch, d in ((A, RIGHT), (A, LEFT), (B, RIGHT), (B, LEFT)):
                last = steps_of(ch, d)
                if s - 1 > last:
                    continue
                o = origin(d, s - 1)
                if s > 1:
                    z_copy(m, ch, d, s - 1, o).wait_recv()
                if s <= last:
                    z_copy(m, ch, d, s, o).start()
                if s > 1 and ch == A:
                    ref = at[m](o, A)
                    remote(ref, ref, z_send.at[m, 2], c_recv.at[m], y_dev).start()

    def z_done(m):
        w = whole[m][A]
        remote(w, w, z_send.at[m, 2], c_recv.at[m], y_dev).wait_recv()

    H0, H1 = pl.ds(0, D // 2), pl.ds(D // 2, D // 2)
    every = pl.ds(0, D)

    def ag(ph, i, xx, cc, cols, dev):
        ref = xg.at[ph, pl.ds(mo((cc * 4 + xx) * T, 16), T), cols]
        return remote(ref, ref, ag_send.at[ph, i], ag_recv.at[ph, i], dev)

    def ag_start(ph):
        ag(ph, 0, xi, ci, H0, x_right).start()
        ag(ph, 3, xi, ci, H1, x_left).start()
        ag(ph, 6, xi, ci, every, mate).start()
        ag(ph, 1, xi, ci, H1, x_right).start()
        ag(ph, 4, xi, ci, H0, x_left).start()

    def ag_mid(ph):
        ag(ph, 0, x3, ci, H0, x_right).wait_recv()
        ag(ph, 2, x3, ci, H0, x_right).start()
        ag(ph, 7, x3, ci, H0, mate).start()
        ag(ph, 3, x1, ci, H1, x_left).wait_recv()
        ag(ph, 5, x1, ci, H1, x_left).start()
        ag(ph, 10, x1, ci, H1, mate).start()

    def ag_end(ph):
        ag(ph, 1, x3, ci, H1, x_right).wait_recv()
        ag(ph, 8, x3, ci, H1, mate).start()
        ag(ph, 4, x1, ci, H0, x_left).wait_recv()
        ag(ph, 11, x1, ci, H0, mate).start()
        ag(ph, 2, x2, ci, H0, x_right).wait_recv()
        ag(ph, 9, x2, ci, H0, mate).start()
        ag(ph, 5, x2, ci, H1, x_left).wait_recv()
        ag(ph, 12, x2, ci, H1, mate).start()
        ag(ph, 6, xi, oc, every, mate).wait_recv()
        for i, xx, cols in ((7, x3, H0), (10, x1, H1), (8, x3, H1), (11, x1, H0), (9, x2, H0), (12, x2, H1)):
            ag(ph, i, xx, oc, cols, mate).wait_recv()

    def ag_sent(ph):
        for i in range(13):
            ag(ph, i, xi, ci, every if i == 6 else H0, mate).wait_send()

    W = D // CHUNKS
    V = W // 2

    def rs(ph, k, i, dev):
        if i == 6:
            src, dst = pp.at[ph, :, pl.ds(k * W, W)], rp.at[ph, :, pl.ds(k * W, W)]
        else:
            src, dst = st.at[ph, i, :, pl.ds(k * V, V)], rt.at[ph, i, :, pl.ds(k * V, V)]
        return remote(src, dst, rs_send.at[ph, k, i], rs_recv.at[ph, k, i], dev)

    rs_dev = (x_right, x_right, x_right, x_left, x_left, x_left, mate)
    my_rows = pl.ds(mo(ci * 4 * T, 16), 4 * T)
    mate_rows = pl.ds(mo(oc * 4 * T, 16), 4 * T)

    def rs_a(ph, k, hid, wt):
        def other(j, _):
            cols = pl.ds(mo(k * W + j * 256, 256), 256)
            pp[ph, :, cols] = dot(hid[mate_rows, :], wt[:, cols]).astype(bf16)
            return 0

        lax.fori_loop(0, W // 256, other, 0)
        rs(ph, k, 6, mate).start()

        def mine(j, _):
            cols = pl.ds(mo(k * W + j * 256, 256), 256)
            sm[:, cols] = dot(hid[my_rows, :], wt[:, cols])
            return 0

        lax.fori_loop(0, W // 256, mine, 0)

    def part(ph, xx, c0):
        rows, cols = pl.ds(mo(xx * T, 16), T), pl.ds(c0, V)
        return sm[rows, cols] + rp[ph, rows, cols].astype(f32)

    def rs_b(ph, k):
        rs(ph, k, 6, mate).wait_recv()
        lo, hi, to = k * W, k * W + V, pl.ds(k * V, V)
        for i, xx, c0 in ((0, x2, lo), (3, x2, hi), (1, x1, hi), (4, x3, lo)):
            st[ph, i, :, to] = part(ph, xx, c0).astype(bf16)
            rs(ph, k, i, rs_dev[i]).start()

    def rs_c(ph, k):
        lo, hi, to = k * W, k * W + V, pl.ds(k * V, V)
        for i, xx, c0 in ((0, x1, lo), (3, x3, hi)):
            rs(ph, k, i, rs_dev[i]).wait_recv()
            st[ph, i + 2, :, to] = (part(ph, xx, c0) + rt[ph, i, :, to].astype(f32)).astype(bf16)
            rs(ph, k, i + 2, rs_dev[i + 2]).start()

    def rs_d(ph, k):
        lo, hi, to = k * W, k * W + V, pl.ds(k * V, V)
        for i in (1, 4, 2, 5):
            rs(ph, k, i, rs_dev[i]).wait_recv()
        br[:, pl.ds(lo, V)] = part(ph, xi, lo) + rt[ph, 2, :, to].astype(f32) + rt[ph, 4, :, to].astype(f32)
        br[:, pl.ds(hi, V)] = part(ph, xi, hi) + rt[ph, 1, :, to].astype(f32) + rt[ph, 5, :, to].astype(f32)

    def rs_sent(ph):
        for k in range(CHUNKS):
            for i in range(7):
                rs(ph, k, i, rs_dev[i]).wait_send()

    def scatter(ph, hid, wt, between):
        for k in range(CHUNKS):
            rs_a(ph, k, hid, wt)
        for stage in (rs_b, rs_c, rs_d):
            for k in range(CHUNKS):
                stage(ph, k)
                between()

    own_rows = pl.ds(mo((ci * 4 + xi) * T, 16), T)

    def post_norm(ph, scale):
        z = GAIN * xg[ph, own_rows, :].astype(f32) + scale * br[...]
        z = z - jnp.mean(z, axis=-1, keepdims=True)
        return (z * lax.rsqrt(jnp.mean(z * z, axis=-1, keepdims=True) + EPS)).astype(bf16)

    def expand(ph, j0, j1):
        def one(j, _):
            p = dot(xg[ph], gu[:, pl.ds(mo(j * 256, 256), 256)])
            gate, up = p[:, 0:128], p[:, 128:256]
            hb[:, pl.ds(mo(j * 128, 128), 128)] = (gate / (1.0 + jnp.exp(-gate)) * up).astype(bf16)
            return 0

        lax.fori_loop(j0, j1, one, 0)

    def setup_attention():
        t = lax.broadcasted_iota(jnp.int32, (128, 256), 0)
        l = lax.broadcasted_iota(jnp.int32, (128, 256), 1)
        is_key = jnp.where(l >= 128, 1, 0)
        s = l - 128 * is_key
        before = (s + is_key) <= t
        after = (s - is_key) >= t
        for p in range(9):
            if p < 7:
                same = (t >> p) == (s >> p)
                odd = ((t >> p) & 1) == 1
                take = same & ((odd & before) | (jnp.logical_not(odd) & after))
            else:
                take = before if p == 7 else after
            mm[p * 128 : p * 128 + 128, :] = jnp.where(take, 1.0, 0.0).astype(bf16)
        for ref in (qk, lg, og, vb):
            for b in range(2):
                ref[b * PAD + SEQ : b * PAD + PAD, :] = jnp.zeros((PAD - SEQ, 128), ref.dtype)
        for h in range(2):
            lanes = slice(h * 64, h * 64 + 64)
            wle2[:, lanes] = wle[...].astype(f32)
            bias2[:, lanes] = bias[...]
            extra2[:, lanes] = extra[...]

    def place(t):
        return (t // 4) * PAD + (t % 4) * T

    def project():
        a = xg[1]
        p1 = dot(a, qb[:, 0:256])
        p2 = dot(a, qb[:, 256:384])
        low = dot(a, wls[...]).astype(bf16)
        pre = dot(low, wle2[...].astype(bf16)) + bias2[...]
        decay = (jnp.minimum(pre, 0.0) - jnp.log1p(jnp.exp(-jnp.abs(pre)))) / STEEP
        for t in range(8):
            src = ((t % 2) * 4 + t // 2) * T
            to = pl.ds(place(t), T)
            qk[to, :] = p1[src : src + T, 0:128].astype(bf16).astype(f32)
            vb[to, :] = p1[src : src + T, 128:256].astype(bf16)
            og[to, :] = p2[src : src + T, :].astype(bf16).astype(f32)
            lg[to, :] = decay[src : src + T, :] + extra2[t * T : t * T + T, :]

    def attend():
        lane = lax.broadcasted_iota(jnp.int32, (128, 128), 1)
        row = lax.broadcasted_iota(jnp.int32, (128, 128), 0)
        is_q = lane < 64
        differ = row ^ lane

        def sequence(b, _):
            heads, tails, totals, vals, diag = [], [], [], [], []
            for c in range(3):
                rows = pl.ds(mo(b * PAD + c * 128, 128), 128)
                both = qk[rows, :]
                g = lg[rows, :]
                hi = g.astype(bf16)
                lo = (g - hi.astype(f32)).astype(bf16)
                zero = jnp.zeros_like(hi)
                top = jnp.concatenate([jnp.where(is_q, hi, zero), jnp.where(is_q, lo, zero)], axis=1)
                bot = jnp.concatenate([jnp.where(is_q, zero, hi), jnp.where(is_q, zero, lo)], axis=1)
                e = dot(mm[...], jnp.concatenate([top, bot], axis=0))
                e = e[:, 0:128] + e[:, 128:256]
                w = jnp.exp(e)

                def pair(scaled):
                    q = jnp.where(is_q, scaled, 0.0).astype(bf16)
                    return q, pltpu.roll(scaled, 64, 1).astype(bf16)

                scores = dot_t(*pair(both))
                for p in range(7):
                    scores = jnp.where(differ >= (1 << p), dot_t(*pair(both * w[p * 128 : p * 128 + 128])), scores)
                diag.append(scores)
                heads.append(pair(both * w[896:1024]))
                tails.append((both, w[1024:1152], e[1024:1152]))
                totals.append(jnp.sum(g, axis=0, keepdims=True))
                vals.append(vb[rows, :])
                if c == 2:
                    tail = [pair(tails[i][0] * tails[i][1]) for i in range(2)]
                    far = pair(tails[0][0] * jnp.exp(tails[0][2] + totals[1]))
            s01 = dot_t(tail[0][0], heads[1][1])
            s10 = dot_t(heads[1][0], tail[0][1])
            s12 = dot_t(tail[1][0], heads[2][1])
            s21 = dot_t(heads[2][0], tail[1][1])
            s02 = dot_t(far[0], heads[2][1])
            s20 = dot_t(heads[2][0], far[1])
            grid = ((diag[0], s01, s02), (s10, diag[1], s12), (s20, s21, diag[2]))
            for c in range(3):
                rows = pl.ds(mo(b * PAD + c * 128, 128), 128)
                o = sum(dot(grid[c][i].astype(bf16), vals[i]) for i in range(3))
                o = o * lax.rsqrt(jnp.mean(o * o, axis=-1, keepdims=True) + EPS) * gain[...]
                gate = og[rows, :]
                qk[rows, :] = o * (gate / (1.0 + jnp.exp(-gate)))
            return 0

        lax.fori_loop(0, 2, sequence, 0)
        for t in range(8):
            dst = ((t % 2) * 4 + t // 2) * T
            gt[dst : dst + T, :] = qk[pl.ds(place(t), T), :].astype(bf16)

    for c in locals_:
        c.wait()
    tick(1)
    ag_start(0)
    setup_attention()
    tick(2)
    ag_mid(0)
    tick(3)
    ag_end(0)
    clock = [4]
    last_tick = max(OFFSETS) + H + 1

    def advance(upto):
        while clock[0] <= min(upto, last_tick):
            tick(clock[0])
            clock[0] += 1

    advance(OFFSETS[0] + H + 1)
    z_done(0)
    expand(0, 0, 2)
    advance(clock[0])
    expand(0, 2, 4)
    advance(clock[0])
    expand(0, 4, 5)
    advance(OFFSETS[1] + H + 1)
    z_done(1)
    scatter(0, hb, dn, lambda: advance(clock[0]))
    y = post_norm(0, 0.5)
    xg[1, own_rows, :] = y
    ag_start(1)
    advance(clock[0])
    ag_mid(1)
    advance(last_tick)
    ag_end(1)
    z_done(2)
    project()
    attend()
    z_done(3)
    scatter(1, gt, ob, lambda: None)
    y = post_norm(1, 1.0)
    xg[2, own_rows, :] = y
    ag_start(2)
    ag_mid(2)
    ag_end(2)
    expand(2, 0, 5)
    scatter(2, hb, dn, lambda: None)
    out[...] = post_norm(2, 0.5)

    for m in range(4):
        for ch, i in ((A, A), (B, B), (A, 2)):
            w = whole[m][ch]
            remote(w, w, z_send.at[m, i], c_recv.at[m], y_dev).wait_send()
    for ph in range(3):
        ag_sent(ph)
        rs_sent(ph)


def solution(mesh):
    n = mesh.shape["fs"]
    assert mesh.shape["grp"] % 2 == 0 and n % 2 == 0 and mesh.shape["tp"] == 8

    def per_device(x, wsw, wex, wct, wq, wk, wv, wg, wls, wle, bias, extra, gain, wo):
        T, D = x.shape
        K, F = wsw.shape
        N8 = 8 * T
        half = D // 2
        vmem = pl.BlockSpec(memory_space=pltpu.VMEM)
        anywhere = pl.BlockSpec(memory_space=pl.ANY)
        dma = pltpu.SemaphoreType.DMA
        return pl.pallas_call(
            functools.partial(kernel, n),
            out_shape=jax.ShapeDtypeStruct((T, D), bf16),
            in_specs=[anywhere] * 4 + [vmem] * 2 + [anywhere] * 2 + [vmem] * 5 + [anywhere],
            out_specs=vmem,
            scratch_shapes=[
                pltpu.VMEM((D, 2 * F), bf16),
                pltpu.VMEM((F, D), bf16),
                pltpu.VMEM((D, 384), bf16),
                pltpu.VMEM((128, D), bf16),
                pltpu.VMEM((3, N8, D), bf16),
                pltpu.VMEM((N8, F), bf16),
                pltpu.VMEM((3, N8 // 2, D), bf16),
                pltpu.VMEM((3, N8 // 2, D), bf16),
                pltpu.VMEM((N8 // 2, D), f32),
                pltpu.VMEM((3, 6, T, half), bf16),
                pltpu.VMEM((3, 6, T, half), bf16),
                pltpu.VMEM((T, D), f32),
                pltpu.VMEM((2 * PAD, 128), f32),
                pltpu.VMEM((2 * PAD, 128), bf16),
                pltpu.VMEM((2 * PAD, 128), f32),
                pltpu.VMEM((2 * PAD, 128), f32),
                pltpu.VMEM((9 * 128, 256), bf16),
                pltpu.VMEM((wle.shape[0], 128), f32),
                pltpu.VMEM((1, 128), f32),
                pltpu.VMEM((N8, 128), f32),
                pltpu.VMEM((N8, 128), bf16),
                dma((4, 2, 2, n // 2)),
                dma((4,)),
                dma((4, 3)),
                dma((3, 13)),
                dma((3, 13)),
                dma((3, CHUNKS, 7)),
                dma((3, CHUNKS, 7)),
                dma((2 * F // 128 + 5,)),
            ],
            compiler_params=pltpu.CompilerParams(
                collective_id=0, has_side_effects=True, vmem_limit_bytes=60 * 1024 * 1024
            ),
        )(x, wsw, wex, wct, wq, wk, wv, wg, wls, wle, bias.reshape(1, -1), extra, gain.reshape(1, -1), wo)

    return jax.shard_map(
        per_device,
        mesh=mesh,
        in_specs=(
            P(("grp", "fs", "tp"), None),
            P("fs", "tp"),
            P("fs", "tp"),
            P("tp", "fs"),
            P("fs", "tp"),
            P("fs", "tp"),
            P("fs", "tp"),
            P("fs", "tp"),
            P(),
            P(None, "tp"),
            P("tp"),
            P(("grp", "fs"), "tp"),
            P(),
            P("tp", "fs"),
        ),
        out_specs=P(("grp", "fs", "tp"), None),
        check_vma=False,
    )
```

time: 504 us -> 197 us (0.39)
  Pallas kernels: 0 us -> 190 us
  waiting for transfers between devices: 163 us -> 0 us
  blocking collectives: 162 us -> 0 us
  matrix products: 67.5 us -> 0 us
  other arithmetic: 40.3 us -> 0 us
  starting transfers between devices: 28 us -> 0 us
  local copies, waits for them, and re-layouts: 25.8 us -> 6.7 us
  between operations: 13.4 us -> 0.01 us
    pallas_call x0 -> x1, Pallas kernels: none -> 190 us  [per_device(): pl.pallas_call(functools.partial(kernel, n), out_shape=jax.ShapeDtypeStru...]
    all_to_all x4 -> x0, blocking collectives: 162 us -> none  [the longest x2 90.3 us: sent_to_all(): return lax.all_to_all(copies, axis, split_axis=0, concat_axis=0, tiled=True)]
    all_gather x3 -> x0, waiting for transfers between devices: 99.9 us -> none  [the longest x1 70.1 us: per_device(): lax.all_gather(perceptron_contract_coefficients, 'fs', axis=1, tiled=True)]
    dot_general x24 -> x0, matrix products: 67.5 us -> none  [the longest x3 27.6 us: return_rows(): jnp.dot(hidden, weight_full, preferred_element_type=jnp.float32)]
    all_to_all x3 -> x0, waiting for transfers between devices: 62.6 us -> none  [the longest x2 31.8 us: sent_to_all(): return lax.all_to_all(copies, axis, split_axis=0, concat_axis=0, tiled=True)]
    all_to_all x3 -> x0, starting transfers between devices: 27.9 us -> none  [the longest x1 16.1 us: sent_and_summed(): lax.all_to_all(tiles, axis, split_axis=0, concat_axis=0, tiled=True)]
    reduce_sum x19 -> x0, other arithmetic: 16.7 us -> none  [the longest x10 14 us: within_block(): jnp.sum(query_one[:, None, :] * key_one[None, :, :] * jnp.exp(spread), ax...]
    while x10 -> x0, other arithmetic: 9.28 us -> none
  transfers between devices with their start and end apart: 6 -> 0, of which waited for: 4 -> 0; matrix products, arithmetic and copies ran while one was open for 19% -> 0% of each run, Pallas kernels for 0% -> 0%
where the time goes in v1:
time: 197 us
  Pallas kernels  190 us (96%)
  local copies, waits for them, and re-layouts  6.7 us (3%)
    pallas_call x1, Pallas kernels, per_device(): pl.pallas_call(functools.partial(kernel, n), out_shape=jax.ShapeDtypeStru...  190 us
    unnamed x9, local copies, waits for them, and re-layouts  6.7 us

profile of v1, /device:TPU:33, one launch (start us, length us, event | category | flops | bytes accessed | tf_op | source)
XLA Modules:
  0.0 196.9 jit_solution(1153274794338843181)
XLA Ops:
  0.0 0.0 copy-start.1
  0.0 1.4 copy.15.wq
  1.4 0.0 copy-done.1
  1.4 0.7 copy.16.wk
  2.1 0.0 copy-start
  2.2 1.8 copy.18.extra
  4.0 0.0 copy-done
  4.0 1.0 copy.17.wls
  5.0 190.2 %shard_map.136 = bf16[80,2048]{1,0:T(8,128)(2,1)} custom-call(bf16[80,2048]{1,0:T(8,128)(2,1)} %x_in.1, bf16[128,640]{1,0:T(8,128)(2,1)} %wsw.1, bf16[128,640]{1,0:T(8,128)(2,1)} %wex.1, bf16[640,128]{1,0:T(8,128)(2,1)} %wct.1, bf16[128,64]{1,0:T(8,128)(2,1)} %copy.15.wq, bf16[128,64]{1,0:T(8,128)(2,1)} %copy.16.wk, bf16[128,128]{1,0:T(8,128)(2,1)} %wv.1, ...), custom_call_target="tpu_custom_call" | custom-call | tf_op jit(solution)/shard_map/pallas_call | solution.py:440
  195.2 1.7 copy.20
Async XLA Ops:
  0.0 1.4 copy-start.1
  2.1 1.8 copy-start

commit v2 on v1

--- a/solution.py
+++ b/solution.py
@@ -15,8 +15,14 @@
 GAIN = 1.681792830507429
 STEEP = 16.0
 EPS = 1e-06
-CHUNKS = 2
-OFFSETS = (0, 3, 6, 6)
+CHUNKS = 4
+OFFSETS = (0, 3, 9, 0)
+NEAR = 5
+FIRST = (
+    "e0 g0 t0", "e1 g1 t0", "w0 o0 m0", "w1 o1 m1 t0", "b0 w2 o2 m2", "b1 w3 o3 m3", "g2 b2 t0",
+    "b3 c0 c1 t0", "c2 c3 t0", "d0 d1 d2 d3",
+)
+STEPS = ("o0 o1 m0 b0", "o2 m1 b1 o3", "m2 b2 m3 c0", "b3 c1 c2 c3", "d0 d1 d2 d3")
 RIGHT, LEFT = 0, 1
 A, B = 0, 1
 f32, bf16 = jnp.float32, jnp.bfloat16
@@ -36,11 +42,12 @@
 
 def kernel(
     n,
-    x_in, wsw, wex, wct, wq, wk, wv, wg, wls, wle, bias, extra, gain, wo,
+    x_in, wsw, wex, wct, wq_t, wk_t, wv, wg, wls_t, wle_in, bias_in, extra_t, gain_in, wo,
     out,
-    gu, dn, qb, ob, xg, hb, pp, rp, sm, st, rt, br,
+    gu, dn, qb, wof, ga, xg, hb, pp, rp, sm, st, rt, br,
     qk, vb, og, lg, mm, wle2, bias2, extra2, gt,
-    z_recv, c_recv, z_send, ag_recv, ag_send, rs_recv, rs_send, loc,
+    wqk, wls, wle, bias, extra, gain,
+    z_recv, c_recv, c_dn, c_ob, z_send, ag_recv, ag_send, rs_recv, rs_send, aa_recv, aa_send, loc,
 ):
     T, D = x_in.shape
     K = wsw.shape[0]
@@ -69,6 +76,11 @@
             src_ref=src, dst_ref=dst, send_sem=s, recv_sem=r, device_id=dev, device_id_type=MESH
         )
 
+    barrier = pltpu.get_barrier_semaphore()
+    others = [{"tp": xx * 2 + cc} for xx in (x1, x2, x3) for cc in (ci, oc)]
+    for dev in (z_right, z_left, y_dev, mate, *others):
+        pl.semaphore_signal(barrier, inc=1, device_id=dev, device_id_type=MESH)
+
     locals_ = []
     own = pl.ds(mo(zi * K, K), K)
     for j in range(F // 128):
@@ -76,20 +88,20 @@
         locals_.append((wsw.at[:, col], gu.at[own, pl.ds(j * 256, 128)]))
         locals_.append((wex.at[:, col], gu.at[own, pl.ds(j * 256 + 128, 128)]))
     locals_.append((x_in, xg.at[0, pl.ds(mo((ci * 4 + xi) * T, 16), T)]))
+    locals_.append((wo, wof.at[pl.ds(mo(ti * 128, 128), 128), pl.ds(NEAR * K, K)]))
+    first = len(locals_)
     locals_.append((wct, dn.at[:, own]))
     locals_.append((wv, qb.at[own, pl.ds(128, 128)]))
     locals_.append((wg, qb.at[own, pl.ds(256, 128)]))
-    locals_.append((wo, ob.at[:, own]))
-    locals_ = [pltpu.make_async_copy(s, d, loc.at[i]) for i, (s, d) in enumerate(locals_)]
+    locals_.append((wq_t, wqk.at[0]))
+    locals_.append((wk_t, wqk.at[1]))
+    locals_ += [(wls_t, wls), (wle_in, wle), (bias_in, bias), (extra_t, extra), (gain_in, gain)]
+    locals_ = [pltpu.make_async_copy(src, dst, loc.at[i]) for i, (src, dst) in enumerate(locals_)]
     for c in locals_:
         c.start()
-    qb[own, 0:64] = wq[...]
-    qb[own, 64:128] = wk[...]
-
-    barrier = pltpu.get_barrier_semaphore()
-    for dev in (z_right, z_left, y_dev, x_right, x_left, mate):
-        pl.semaphore_signal(barrier, inc=1, device_id=dev, device_id_type=MESH)
-    pl.semaphore_wait(barrier, 6)
+    for c in locals_[:first]:
+        c.wait()
+    pl.semaphore_wait(barrier, 10)
 
     def rows_of(o):
         return pl.ds(mo(o * K, K), K)
@@ -103,8 +115,12 @@
     def qb_at(o, ch):
         return qb.at[rows_of(o), pl.ds(mo(par * 256, 128), 128) if ch == A else pl.ds(128, 128)]
 
-    def ob_at(o, ch):
-        return ob.at[pl.ds(mo(par * 80, 16), 48) if ch == A else pl.ds(48, 32), rows_of(o)]
+    def ob_at(slot, ch):
+        rows = mo(ti * 128 + par * 80, 16) if ch == A else mo(ti * 128 + 48, 16)
+        return wof.at[pl.ds(rows, 48 if ch == A else 32), pl.ds(slot * K, K)]
+
+    def ob_slot(d, dist):
+        return (NEAR - dist) % n if d == RIGHT else (NEAR + dist) % n
 
     at = (gu_at, dn_at, qb_at, ob_at)
     R = (n - 1) * K
@@ -112,7 +128,7 @@
         (gu.at[0:R, 0:384], gu.at[0:R, 384:896]),
         (dn.at[0:208, 0:R], dn.at[208:432, 0:R]),
         (qb.at[0:R, 0:128], qb.at[0:R, 128:256]),
-        (ob.at[0:48, 0:R], ob.at[48:80, 0:R]),
+        (wof.at[0:48, 0:R], wof.at[48:80, 0:R]),
     )
 
     def steps_of(ch, d):
@@ -122,8 +138,11 @@
         return lax.rem(zi + n - back, n) if d == RIGHT else lax.rem(zi + back, n)
 
     def z_copy(m, ch, d, s, o):
-        ref = at[m](o, ch)
-        return remote(ref, ref, z_send.at[m, ch], z_recv.at[m, d, ch, s - 1], z_dev[d])
+        if m == 3:
+            src, dst = ob_at(ob_slot(d, s - 1), ch), ob_at(ob_slot(d, s), ch)
+        else:
+            src = dst = at[m](o, ch)
+        return remote(src, dst, z_send.at[m, ch], z_recv.at[m, d, ch, s - 1], z_dev[d])
 
     def tick(t):
         for m in range(4):
@@ -140,19 +159,45 @@
                 if s <= last:
                     z_copy(m, ch, d, s, o).start()
                 if s > 1 and ch == A:
-                    ref = at[m](o, A)
-                    remote(ref, ref, z_send.at[m, 2], c_recv.at[m], y_dev).start()
+                    ref = ob_at(ob_slot(d, s - 1), A) if m == 3 else at[m](o, A)
+                    landed = c_recv.at[m]
+                    if m == 1:
+                        landed = c_dn.at[s - 2, d]
+                    elif m == 3:
+                        landed = c_ob.at[0 if s - 1 <= NEAR else 1]
+                    remote(ref, ref, z_send.at[m, 2], landed, y_dev).start()
 
     def z_done(m):
         w = whole[m][A]
         remote(w, w, z_send.at[m, 2], c_recv.at[m], y_dev).wait_recv()
 
+    def dn_done(dist, d):
+        ref = dn_at(zi, A)
+        remote(ref, ref, z_send.at[1, 2], c_dn.at[dist - 1, d], y_dev).wait_recv()
+
+    def ob_done(batch):
+        ref = wof.at[0:48, 0 : (2 * NEAR if batch == 0 else n - 1 - 2 * NEAR) * K]
+        remote(ref, ref, z_send.at[3, 2], c_ob.at[batch], y_dev).wait_recv()
+
+    def z_sent(m):
+        for ch, i in ((A, A), (B, B), (A, 2)):
+            w = whole[m][ch]
+            remote(w, w, z_send.at[m, i], c_recv.at[m], y_dev).wait_send()
+
     H0, H1 = pl.ds(0, D // 2), pl.ds(D // 2, D // 2)
     every = pl.ds(0, D)
 
+    near_cols = (2 * NEAR + 1) * K
+    batches = ((0, 6 * K, near_cols), (near_cols, near_cols + 3 * K, D))
+
     def ag(ph, i, xx, cc, cols, dev):
-        ref = xg.at[ph, pl.ds(mo((cc * 4 + xx) * T, 16), T), cols]
-        return remote(ref, ref, ag_send.at[ph, i], ag_recv.at[ph, i], dev)
+        if ph < 3:
+            ref = xg.at[ph, pl.ds(mo((cc * 4 + xx) * T, 16), T), cols]
+        else:
+            lo, mid, hi = batches[ph - 3]
+            cols = pl.ds(lo, mid - lo) if cols is H0 else pl.ds(mid, hi - mid) if cols is H1 else pl.ds(lo, hi - lo)
+            ref = wof.at[pl.ds(mo((xx * 2 + cc) * 128, 128), 128), cols]
+        return remote(ref, ref, ag_send.at[ph], ag_recv.at[ph, i], dev)
 
     def ag_start(ph):
         ag(ph, 0, xi, ci, H0, x_right).start()
@@ -169,22 +214,28 @@
         ag(ph, 5, x1, ci, H1, x_left).start()
         ag(ph, 10, x1, ci, H1, mate).start()
 
-    def ag_end(ph):
+    def ag_near(ph):
         ag(ph, 1, x3, ci, H1, x_right).wait_recv()
         ag(ph, 8, x3, ci, H1, mate).start()
         ag(ph, 4, x1, ci, H0, x_left).wait_recv()
         ag(ph, 11, x1, ci, H0, mate).start()
+        ag(ph, 6, xi, oc, every, mate).wait_recv()
+        for i, xx, cols in ((7, x3, H0), (10, x1, H1), (8, x3, H1), (11, x1, H0)):
+            ag(ph, i, xx, oc, cols, mate).wait_recv()
+
+    def ag_far(ph):
         ag(ph, 2, x2, ci, H0, x_right).wait_recv()
         ag(ph, 9, x2, ci, H0, mate).start()
         ag(ph, 5, x2, ci, H1, x_left).wait_recv()
         ag(ph, 12, x2, ci, H1, mate).start()
-        ag(ph, 6, xi, oc, every, mate).wait_recv()
-        for i, xx, cols in ((7, x3, H0), (10, x1, H1), (8, x3, H1), (11, x1, H0), (9, x2, H0), (12, x2, H1)):
-            ag(ph, i, xx, oc, cols, mate).wait_recv()
+
+    def ag_end(ph):
+        ag(ph, 9, x2, oc, H0, mate).wait_recv()
+        ag(ph, 12, x2, oc, H1, mate).wait_recv()
 
     def ag_sent(ph):
-        for i in range(13):
-            ag(ph, i, xi, ci, every if i == 6 else H0, mate).wait_send()
+        ref = xg.at[ph, 0 : 7 * T] if ph < 3 else wof.at[0 : 7 * 128, batches[ph - 3][0] : batches[ph - 3][2]]
+        remote(ref, ref, ag_send.at[ph], ag_recv.at[ph, 0], mate).wait_send()
 
     W = D // CHUNKS
     V = W // 2
@@ -194,27 +245,34 @@
             src, dst = pp.at[ph, :, pl.ds(k * W, W)], rp.at[ph, :, pl.ds(k * W, W)]
         else:
             src, dst = st.at[ph, i, :, pl.ds(k * V, V)], rt.at[ph, i, :, pl.ds(k * V, V)]
-        return remote(src, dst, rs_send.at[ph, k, i], rs_recv.at[ph, k, i], dev)
+        return remote(src, dst, rs_send.at[ph, i // 6], rs_recv.at[ph, k, i], dev)
 
     rs_dev = (x_right, x_right, x_right, x_left, x_left, x_left, mate)
     my_rows = pl.ds(mo(ci * 4 * T, 16), 4 * T)
     mate_rows = pl.ds(mo(oc * 4 * T, 16), 4 * T)
 
-    def rs_a(ph, k, hid, wt):
-        def other(j, _):
-            cols = pl.ds(mo(k * W + j * 256, 256), 256)
-            pp[ph, :, cols] = dot(hid[mate_rows, :], wt[:, cols]).astype(bf16)
-            return 0
-
-        lax.fori_loop(0, W // 256, other, 0)
+    order = [(0, RIGHT)] + [(j // 2 + 1, j % 2) for j in range(n - 1)]
+    BLOCKS = W // K
+
+    def columns(ph, slot):
+        if ph == 0:
+            dist, d = order[slot]
+            return pl.ds(mo(origin(d, dist) * K, K), K)
+        return pl.ds(slot * K, K)
+
+    def two_blocks(ph, wt, slot):
+        if ph == 0:
+            return jnp.concatenate([wt[:, columns(ph, slot)], wt[:, columns(ph, slot + 1)]], axis=1)
+        return wt[:, pl.ds(slot * K, 2 * K)]
+
+    def rs_o(ph, k, hid, wt):
+        for slot in range(k * BLOCKS, (k + 1) * BLOCKS, 2):
+            pp[ph, :, pl.ds(slot * K, 2 * K)] = dot(hid[mate_rows, :], two_blocks(ph, wt, slot)).astype(bf16)
         rs(ph, k, 6, mate).start()
 
-        def mine(j, _):
-            cols = pl.ds(mo(k * W + j * 256, 256), 256)
-            sm[:, cols] = dot(hid[my_rows, :], wt[:, cols])
-            return 0
-
-        lax.fori_loop(0, W // 256, mine, 0)
+    def rs_m(ph, k, hid, wt):
+        for slot in range(k * BLOCKS, (k + 1) * BLOCKS, 2):
+            sm[:, pl.ds(slot * K, 2 * K)] = dot(hid[my_rows, :], two_blocks(ph, wt, slot))
 
     def part(ph, xx, c0):
         rows, cols = pl.ds(mo(xx * T, 16), T), pl.ds(c0, V)
@@ -238,21 +296,28 @@
         lo, hi, to = k * W, k * W + V, pl.ds(k * V, V)
         for i in (1, 4, 2, 5):
             rs(ph, k, i, rs_dev[i]).wait_recv()
-        br[:, pl.ds(lo, V)] = part(ph, xi, lo) + rt[ph, 2, :, to].astype(f32) + rt[ph, 4, :, to].astype(f32)
-        br[:, pl.ds(hi, V)] = part(ph, xi, hi) + rt[ph, 1, :, to].astype(f32) + rt[ph, 5, :, to].astype(f32)
+        low = part(ph, xi, lo) + rt[ph, 2, :, to].astype(f32) + rt[ph, 4, :, to].astype(f32)
+        high = part(ph, xi, hi) + rt[ph, 1, :, to].astype(f32) + rt[ph, 5, :, to].astype(f32)
+        for i in range(BLOCKS // 2):
+            br[:, columns(ph, k * BLOCKS + i)] = low[:, i * K : i * K + K]
+            br[:, columns(ph, k * BLOCKS + BLOCKS // 2 + i)] = high[:, i * K : i * K + K]
 
     def rs_sent(ph):
-        for k in range(CHUNKS):
-            for i in range(7):
-                rs(ph, k, i, rs_dev[i]).wait_send()
-
-    def scatter(ph, hid, wt, between):
-        for k in range(CHUNKS):
-            rs_a(ph, k, hid, wt)
-        for stage in (rs_b, rs_c, rs_d):
-            for k in range(CHUNKS):
-                stage(ph, k)
-                between()
+        for i, ref in ((0, st.at[ph]), (1, pp.at[ph])):
+            remote(ref, ref, rs_send.at[ph, i], rs_recv.at[ph, 0, 0], mate).wait_send()
+
+    def run(ph, hid, wt, steps, clock=None):
+        for step in " ".join(steps).split():
+            what, k = step[0], int(step[1:])
+            with jax.named_scope(f"rs{ph}_{step}"):
+                if what in "wteg":
+                    clock(what, k)
+                elif what == "o":
+                    rs_o(ph, k, hid, wt)
+                elif what == "m":
+                    rs_m(ph, k, hid, wt)
+                else:
+                    {"b": rs_b, "c": rs_c, "d": rs_d}[what](ph, k)
 
     own_rows = pl.ds(mo((ci * 4 + xi) * T, 16), T)
 
@@ -261,11 +326,26 @@
         z = z - jnp.mean(z, axis=-1, keepdims=True)
         return (z * lax.rsqrt(jnp.mean(z * z, axis=-1, keepdims=True) + EPS)).astype(bf16)
 
-    def expand(ph, j0, j1):
+    def rows_at(cc, xx):
+        return pl.ds(mo((cc * 4 + xx) * T, 16), T)
+
+    def expand(ph, j0, j1, chips=None):
+        where = None if chips is None else [rows_at(cc, xx) for xx in chips for cc in (0, 1)]
+
         def one(j, _):
-            p = dot(xg[ph], gu[:, pl.ds(mo(j * 256, 256), 256)])
+            w = gu[:, pl.ds(mo(j * 256, 256), 256)]
+            to = pl.ds(mo(j * 128, 128), 128)
+            if where is None:
+                p = dot(xg[ph], w)
+            else:
+                p = dot(jnp.concatenate([xg[ph, r, :] for r in where], axis=0), w)
             gate, up = p[:, 0:128], p[:, 128:256]
-            hb[:, pl.ds(mo(j * 128, 128), 128)] = (gate / (1.0 + jnp.exp(-gate)) * up).astype(bf16)
+            h = (gate / (1.0 + jnp.exp(-gate)) * up).astype(bf16)
+            if where is None:
+                hb[:, to] = h
+            else:
+                for i, r in enumerate(where):
+                    hb[r, to] = h[i * T : i * T + T, :]
             return 0
 
         lax.fori_loop(j0, j1, one, 0)
@@ -292,33 +372,30 @@
             lanes = slice(h * 64, h * 64 + 64)
             wle2[:, lanes] = wle[...].astype(f32)
             bias2[:, lanes] = bias[...]
-            extra2[:, lanes] = extra[...]
-
-    def place(t):
-        return (t // 4) * PAD + (t % 4) * T
-
-    def project():
-        a = xg[1]
+            qb[own, lanes] = wqk[h].astype(f32).T.astype(bf16)
+            for i in range(8 * T // 128):
+                extra2[i * 128 : i * 128 + 128, lanes] = extra[:, i * 128 : i * 128 + 128].T
+
+    def project(b):
+        seq = [rows_at(i % 2, 2 * b + i // 2) for i in range(4)]
+        a = jnp.concatenate([xg[1, r, :] for r in seq], axis=0)
+        to = pl.ds(mo(b * PAD, 128), SEQ)
         p1 = dot(a, qb[:, 0:256])
-        p2 = dot(a, qb[:, 256:384])
-        low = dot(a, wls[...]).astype(bf16)
+        qk[to, :] = p1[:, 0:128].astype(bf16).astype(f32)
+        vb[to, :] = p1[:, 128:256].astype(bf16)
+        og[to, :] = dot(a, qb[:, 256:384]).astype(bf16).astype(f32)
+        low = dot_t(a, wls[...]).astype(bf16)
         pre = dot(low, wle2[...].astype(bf16)) + bias2[...]
         decay = (jnp.minimum(pre, 0.0) - jnp.log1p(jnp.exp(-jnp.abs(pre)))) / STEEP
-        for t in range(8):
-            src = ((t % 2) * 4 + t // 2) * T
-            to = pl.ds(place(t), T)
-            qk[to, :] = p1[src : src + T, 0:128].astype(bf16).astype(f32)
-            vb[to, :] = p1[src : src + T, 128:256].astype(bf16)
-            og[to, :] = p2[src : src + T, :].astype(bf16).astype(f32)
-            lg[to, :] = decay[src : src + T, :] + extra2[t * T : t * T + T, :]
-
-    def attend():
+        lg[to, :] = decay + extra2[pl.ds(mo(b * SEQ, 16), SEQ), :]
+
+    def attend(b):
         lane = lax.broadcasted_iota(jnp.int32, (128, 128), 1)
         row = lax.broadcasted_iota(jnp.int32, (128, 128), 0)
         is_q = lane < 64
         differ = row ^ lane
 
-        def sequence(b, _):
+        def sequence():
             heads, tails, totals, vals, diag = [], [], [], [], []
             for c in range(3):
                 rows = pl.ds(mo(b * PAD + c * 128, 128), 128)
@@ -361,68 +438,166 @@
                 o = o * lax.rsqrt(jnp.mean(o * o, axis=-1, keepdims=True) + EPS) * gain[...]
                 gate = og[rows, :]
                 qk[rows, :] = o * (gate / (1.0 + jnp.exp(-gate)))
-            return 0
-
-        lax.fori_loop(0, 2, sequence, 0)
-        for t in range(8):
-            dst = ((t % 2) * 4 + t // 2) * T
-            gt[dst : dst + T, :] = qk[pl.ds(place(t), T), :].astype(bf16)
-
-    for c in locals_:
+
+        sequence()
+        for i in range(4):
+            gt[rows_at(i % 2, 2 * b + i // 2), :] = qk[pl.ds(mo(b * PAD + i * T, 16), T), :].astype(bf16)
+
+    my_cols = pl.ds(mo(ti * 128, 128), 128)
+
+    def hand_out(i, targets):
+        for xx, cc in targets:
+            remote(gt.at[rows_at(cc, xx)], ga.at[:, my_cols], aa_send.at[i], aa_recv.at[i], {"tp": xx * 2 + cc}).start()
+
+    def handed(i, count):
+        ref = gt.at[0 : count * T]
+        return remote(ref, ref, aa_send.at[i], aa_recv.at[i], mate)
+
+    def emit():
+        for slot in range(0, n, 2):
+            p = dot(ga[...], wof[:, slot * K : slot * K + 2 * K])
+            for i in range(2):
+                o = lax.rem(zi + n + slot + i - NEAR, n)
+                br[:, rows_of(o)] = p[:, i * K : i * K + K]
+
+    at_tick = [1]
+    last_tick = max(OFFSETS) + H + 1
+    scope = jax.named_scope
+
+    def advance(upto):
+        while at_tick[0] <= min(upto, last_tick):
+            with scope(f"tick_{at_tick[0]}"):
+                tick(at_tick[0])
+            at_tick[0] += 1
+
+    def landed(k):
+        advance(OFFSETS[1] + 2 * k + 3)
+        with scope("dn_done"):
+            for dist, d in order[max(1, 4 * k) : 4 * k + 4]:
+                dn_done(dist, d)
+
+    def more(count):
+        advance(at_tick[0] + count - 1)
+
+    advance(1)
+    ag_start(0)
+    for c in locals_[first:]:
         c.wait()
-    tick(1)
-    ag_start(0)
-    setup_attention()
-    tick(2)
-    ag_mid(0)
-    tick(3)
+    with scope("setup"):
+        setup_attention()
+    advance(2)
+    with scope("ag0_mid"):
+        ag_mid(0)
+    advance(3)
+    with scope("ag0_near"):
+        ag_near(0)
+    with scope("ag0_far"):
+        ag_far(0)
+    advance(4)
     ag_end(0)
-    clock = [4]
-    last_tick = max(OFFSETS) + H + 1
-
-    def advance(upto):
-        while clock[0] <= min(upto, last_tick):
-            tick(clock[0])
-            clock[0] += 1
-
+    advance(NEAR + 2)
+    with scope("ob_near"):
+        ob_done(0)
+        ag_start(3)
+    advance(NEAR + 3)
+    with scope("ob_mid"):
+        ag_mid(3)
     advance(OFFSETS[0] + H + 1)
-    z_done(0)
-    expand(0, 0, 2)
-    advance(clock[0])
-    expand(0, 2, 4)
-    advance(clock[0])
-    expand(0, 4, 5)
-    advance(OFFSETS[1] + H + 1)
-    z_done(1)
-    scatter(0, hb, dn, lambda: advance(clock[0]))
-    y = post_norm(0, 0.5)
-    xg[1, own_rows, :] = y
+    with scope("ob_far"):
+        ag_near(3)
+        ag_far(3)
+    with scope("gu_done"):
+        z_done(0)
+
+    def other(what, k):
+        if what == "w":
+            landed(k)
+        elif what == "t":
+            more(1)
+        elif what == "g":
+            if k == 0:
+                ob_done(1)
+                ag_start(4)
+            elif k == 1:
+                ag_mid(4)
+            else:
+                ag_near(4)
+                ag_far(4)
+        else:
+            expand(0, 3 * k, 3 + 2 * k)
+
+    run(0, hb, dn, FIRST, other)
+    with scope("norm"):
+        xg[1, own_rows, :] = post_norm(0, 0.5)
     ag_start(1)
-    advance(clock[0])
-    ag_mid(1)
+    z_sent(0)
+    z_sent(1)
+    ag_sent(0)
+    more(1)
+    with scope("ag1_mid"):
+        ag_mid(1)
     advance(last_tick)
-    ag_end(1)
-    z_done(2)
-    project()
-    attend()
-    z_done(3)
-    scatter(1, gt, ob, lambda: None)
-    y = post_norm(1, 1.0)
-    xg[2, own_rows, :] = y
+    with scope("ag1_near"):
+        ag_near(1)
+    with scope("qb_done"):
+        z_done(2)
+    seq = lax.div(xi, 2)
+    pair = xi + 1 - 2 * lax.rem(xi, 2)
+    away = 2 * (1 - seq)
+    with scope("project"):
+        project(seq)
+    with scope("ag1_far"):
+        ag_far(1)
+    with scope("attend"):
+        attend(seq)
+        hand_out(0, ((pair, ci), (pair, oc), (xi, oc)))
+    with scope("ag1_end"):
+        ag_end(1)
+    with scope("project"):
+        project(1 - seq)
+    with scope("attend"):
+        attend(1 - seq)
+        hand_out(1, ((away, 0), (away, 1), (away + 1, 0), (away + 1, 1)))
+    ga[:, my_cols] = gt[own_rows, :]
+    with scope("ob_end"):
+        ag_end(3)
+        ag_end(4)
+    with scope("handed"):
+        handed(0, 3).wait_recv()
+        handed(1, 4).wait_recv()
+    with scope("emit"):
+        emit()
+    with scope("norm"):
+        xg[2, own_rows, :] = post_norm(1, 1.0)
     ag_start(2)
-    ag_mid(2)
-    ag_end(2)
-    expand(2, 0, 5)
-    scatter(2, hb, dn, lambda: None)
-    out[...] = post_norm(2, 0.5)
-
-    for m in range(4):
-        for ch, i in ((A, A), (B, B), (A, 2)):
-            w = whole[m][ch]
-            remote(w, w, z_send.at[m, i], c_recv.at[m], y_dev).wait_send()
-    for ph in range(3):
-        ag_sent(ph)
-        rs_sent(ph)
+    z_sent(2)
+    z_sent(3)
+    rs_sent(0)
+    for i in (1, 3, 4):
+        ag_sent(i)
+    handed(0, 3).wait_send()
+    handed(1, 4).wait_send()
+    with scope("ag2_mid"):
+        ag_mid(2)
+    with scope("ag2_near"):
+        ag_near(2)
+    near = (xi, x1, x3)
+    with scope("expand_near"):
+        expand(2, 0, 3, near)
+    with scope("ag2_far"):
+        ag_far(2)
+    with scope("expand_near"):
+        expand(2, 3, 5, near)
+    with scope("ag2_end"):
+        ag_end(2)
+    with scope("expand_far"):
+        expand(2, 0, 5, (x2,))
+    run(1, hb, dn, STEPS)
+    with scope("norm"):
+        out[...] = post_norm(2, 0.5)
+    with scope("sent"):
+        ag_sent(2)
+        rs_sent(1)
 
 
 def solution(mesh):
@@ -440,20 +615,21 @@
         return pl.pallas_call(
             functools.partial(kernel, n),
             out_shape=jax.ShapeDtypeStruct((T, D), bf16),
-            in_specs=[anywhere] * 4 + [vmem] * 2 + [anywhere] * 2 + [vmem] * 5 + [anywhere],
+            in_specs=[anywhere] * 14,
             out_specs=vmem,
             scratch_shapes=[
                 pltpu.VMEM((D, 2 * F), bf16),
                 pltpu.VMEM((F, D), bf16),
                 pltpu.VMEM((D, 384), bf16),
-                pltpu.VMEM((128, D), bf16),
+                pltpu.VMEM((8 * 128, D), bf16),
+                pltpu.VMEM((T, 8 * 128), bf16),
                 pltpu.VMEM((3, N8, D), bf16),
                 pltpu.VMEM((N8, F), bf16),
-                pltpu.VMEM((3, N8 // 2, D), bf16),
-                pltpu.VMEM((3, N8 // 2, D), bf16),
+                pltpu.VMEM((2, N8 // 2, D), bf16),
+                pltpu.VMEM((2, N8 // 2, D), bf16),
                 pltpu.VMEM((N8 // 2, D), f32),
-                pltpu.VMEM((3, 6, T, half), bf16),
-                pltpu.VMEM((3, 6, T, half), bf16),
+                pltpu.VMEM((2, 6, T, half), bf16),
+                pltpu.VMEM((2, 6, T, half), bf16),
                 pltpu.VMEM((T, D), f32),
                 pltpu.VMEM((2 * PAD, 128), f32),
                 pltpu.VMEM((2 * PAD, 128), bf16),
@@ -464,19 +640,31 @@
                 pltpu.VMEM((1, 128), f32),
                 pltpu.VMEM((N8, 128), f32),
                 pltpu.VMEM((N8, 128), bf16),
+                pltpu.VMEM((2, wq.shape[1], K), bf16),
+                pltpu.VMEM((wls.shape[1], D), bf16),
+                pltpu.VMEM(wle.shape, bf16),
+                pltpu.VMEM((1, bias.shape[0]), f32),
+                pltpu.VMEM((extra.shape[1], extra.shape[0]), f32),
+                pltpu.VMEM((1, gain.shape[0]), f32),
                 dma((4, 2, 2, n // 2)),
                 dma((4,)),
+                dma((n // 2, 2)),
+                dma((2,)),
                 dma((4, 3)),
-                dma((3, 13)),
-                dma((3, 13)),
-                dma((3, CHUNKS, 7)),
-                dma((3, CHUNKS, 7)),
-                dma((2 * F // 128 + 5,)),
+                dma((5, 13)),
+                dma((5,)),
+                dma((2, CHUNKS, 7)),
+                dma((2, 2)),
+                dma((2,)),
+                dma((2,)),
+                dma((2 * F // 128 + 12,)),
             ],
             compiler_params=pltpu.CompilerParams(
                 collective_id=0, has_side_effects=True, vmem_limit_bytes=60 * 1024 * 1024
             ),
-        )(x, wsw, wex, wct, wq, wk, wv, wg, wls, wle, bias.reshape(1, -1), extra, gain.reshape(1, -1), wo)
+        )(
+            x, wsw, wex, wct, wq.T, wk.T, wv, wg, wls.T, wle, bias.reshape(1, -1), extra.T, gain.reshape(1, -1), wo
+        )
 
     return jax.shard_map(
         per_device,

time: 197 us -> 171 us (0.87)
  Pallas kernels: 190 us -> 169 us
  local copies, waits for them, and re-layouts: 6.7 us -> 1.72 us
    pallas_call x1, Pallas kernels: 190 us -> 169 us  [per_device(): pl.pallas_call(functools.partial(kernel, n), out_shape=jax.ShapeDtypeStru...]
    unnamed x9 -> x1, local copies, waits for them, and re-layouts: 6.7 us -> 1.72 us
where the time goes in v2:
time: 171 us
  Pallas kernels  169 us (99%)
  local copies, waits for them, and re-layouts  1.72 us (1%)
    pallas_call x1, Pallas kernels, per_device(): pl.pallas_call(functools.partial(kernel, n), out_shape=jax.ShapeDtypeStru...  169 us

profile of v2, /device:TPU:33, one launch (start us, length us, event | category | flops | bytes accessed | tf_op | source)
XLA Modules:
  0.0 170.6 jit_solution(13754945682205879662)
XLA Ops:
  0.0 168.9 %shard_map.136 = bf16[80,2048]{1,0:T(8,128)(2,1)} custom-call(bf16[80,2048]{1,0:T(8,128)(2,1)} %x_in.1, bf16[128,640]{1,0:T(8,128)(2,1)} %wsw.1, bf16[128,640]{1,0:T(8,128)(2,1)} %wex.1, bf16[640,128]{1,0:T(8,128)(2,1)} %wct.1, bf16[64,128]{1,0:T(8,128)(2,1)} %bitcast.8, bf16[64,128]{1,0:T(8,128)(2,1)} %bitcast.9, bf16[128,128]{1,0:T(8,128)(2,1)} %wv.1, ...), custom_call_target="tpu_custom_call" | custom-call | tf_op jit(solution)/shard_map/pallas_call | solution.py:615
  168.9 1.7 %copy.16 = bf16[80,2048]{1,0:T(8,128)(2,1)} copy(bf16[80,2048]{1,0:T(8,128)(2,1)} %shard_map.136) | data formatting | bytes 655360

commit v3 on v2

--- a/solution.py
+++ b/solution.py
@@ -19,8 +19,8 @@
 OFFSETS = (0, 3, 9, 0)
 NEAR = 5
 FIRST = (
-    "e0 g0 t0", "e1 g1 t0", "w0 o0 m0", "w1 o1 m1 t0", "b0 w2 o2 m2", "b1 w3 o3 m3", "g2 b2 t0",
-    "b3 c0 c1 t0", "c2 c3 t0", "d0 d1 d2 d3",
+    "t0 w0 o0 m0", "w1 o1 m1 t0", "b0 b1 w2 o2", "m2 t0 b2 c0", "c1 w3 o3 m3", "b3 c2 t0 g2",
+    "c3 d0 d1 t0", "d2 d3",
 )
 STEPS = ("o0 o1 m0 b0", "o2 m1 b1 o3", "m2 b2 m3 c0", "b3 c1 c2 c3", "d0 d1 d2 d3")
 RIGHT, LEFT = 0, 1
@@ -44,10 +44,10 @@
     n,
     x_in, wsw, wex, wct, wq_t, wk_t, wv, wg, wls_t, wle_in, bias_in, extra_t, gain_in, wo,
     out,
-    gu, dn, qb, wof, ga, xg, hb, pp, rp, sm, st, rt, br,
+    gu, dn, qb, wof, ga, xg, acc, hb, pp, rp, sm, st, rt, br,
     qk, vb, og, lg, mm, wle2, bias2, extra2, gt,
     wqk, wls, wle, bias, extra, gain,
-    z_recv, c_recv, c_dn, c_ob, z_send, ag_recv, ag_send, rs_recv, rs_send, aa_recv, aa_send, loc,
+    z_recv, c_gu, c_dn, c_qb, c_ob, z_send, ag_recv, ag_send, rs_recv, rs_send, aa_recv, aa_send, loc,
 ):
     T, D = x_in.shape
     K = wsw.shape[0]
@@ -85,8 +85,8 @@
     own = pl.ds(mo(zi * K, K), K)
     for j in range(F // 128):
         col = slice(j * 128, j * 128 + 128)
-        locals_.append((wsw.at[:, col], gu.at[own, pl.ds(j * 256, 128)]))
-        locals_.append((wex.at[:, col], gu.at[own, pl.ds(j * 256 + 128, 128)]))
+        pltpu.make_async_copy(wsw.at[:, col], gu.at[own, pl.ds(j * 256, 128)], loc.at[12]).start()
+        pltpu.make_async_copy(wex.at[:, col], gu.at[own, pl.ds(j * 256 + 128, 128)], loc.at[12]).start()
     locals_.append((x_in, xg.at[0, pl.ds(mo((ci * 4 + xi) * T, 16), T)]))
     locals_.append((wo, wof.at[pl.ds(mo(ti * 128, 128), 128), pl.ds(NEAR * K, K)]))
     first = len(locals_)
@@ -101,6 +101,7 @@
         c.start()
     for c in locals_[:first]:
         c.wait()
+    pltpu.make_async_copy(gu.at[own], gu.at[own], loc.at[12]).wait()
     pl.semaphore_wait(barrier, 10)
 
     def rows_of(o):
@@ -142,7 +143,7 @@
             src, dst = ob_at(ob_slot(d, s - 1), ch), ob_at(ob_slot(d, s), ch)
         else:
             src = dst = at[m](o, ch)
-        return remote(src, dst, z_send.at[m, ch], z_recv.at[m, d, ch, s - 1], z_dev[d])
+        return remote(src, dst, z_send.at[m, ch], z_recv.at[(0, 1, 0, 2)[m], d, ch, s - 1], z_dev[d])
 
     def tick(t):
         for m in range(4):
@@ -160,20 +161,20 @@
                     z_copy(m, ch, d, s, o).start()
                 if s > 1 and ch == A:
                     ref = ob_at(ob_slot(d, s - 1), A) if m == 3 else at[m](o, A)
-                    landed = c_recv.at[m]
-                    if m == 1:
-                        landed = c_dn.at[s - 2, d]
-                    elif m == 3:
-                        landed = c_ob.at[0 if s - 1 <= NEAR else 1]
+                    landed = (c_gu.at[s - 2], c_dn.at[s - 2], c_qb.at[0], c_ob.at[0 if s - 1 <= NEAR else 1])[m]
                     remote(ref, ref, z_send.at[m, 2], landed, y_dev).start()
 
-    def z_done(m):
-        w = whole[m][A]
-        remote(w, w, z_send.at[m, 2], c_recv.at[m], y_dev).wait_recv()
-
-    def dn_done(dist, d):
-        ref = dn_at(zi, A)
-        remote(ref, ref, z_send.at[1, 2], c_dn.at[dist - 1, d], y_dev).wait_recv()
+    def qb_done():
+        w = whole[2][A]
+        remote(w, w, z_send.at[2, 2], c_qb.at[0], y_dev).wait_recv()
+
+    def gu_done(dist):
+        ref = gu.at[0 : (2 if dist < H else 1) * K, 0:384]
+        remote(ref, ref, z_send.at[0, 2], c_gu.at[dist - 1], y_dev).wait_recv()
+
+    def dn_done(dist):
+        ref = dn.at[0:208, 0 : (2 if dist < H else 1) * K]
+        remote(ref, ref, z_send.at[1, 2], c_dn.at[dist - 1], y_dev).wait_recv()
 
     def ob_done(batch):
         ref = wof.at[0:48, 0 : (2 * NEAR if batch == 0 else n - 1 - 2 * NEAR) * K]
@@ -182,7 +183,7 @@
     def z_sent(m):
         for ch, i in ((A, A), (B, B), (A, 2)):
             w = whole[m][ch]
-            remote(w, w, z_send.at[m, i], c_recv.at[m], y_dev).wait_send()
+            remote(w, w, z_send.at[m, i], c_qb.at[0], y_dev).wait_send()
 
     H0, H1 = pl.ds(0, D // 2), pl.ds(D // 2, D // 2)
     every = pl.ds(0, D)
@@ -197,7 +198,13 @@
             lo, mid, hi = batches[ph - 3]
             cols = pl.ds(lo, mid - lo) if cols is H0 else pl.ds(mid, hi - mid) if cols is H1 else pl.ds(lo, hi - lo)
             ref = wof.at[pl.ds(mo((xx * 2 + cc) * 128, 128), 128), cols]
-        return remote(ref, ref, ag_send.at[ph], ag_recv.at[ph, i], dev)
+        slot = i if i < 7 else 8 if i in (9, 12) else 7
+        return remote(ref, ref, ag_send.at[ph], ag_recv.at[ph, slot], dev)
+
+    def from_mate(ph, slot, count):
+        rows = count * (T if ph < 3 else 128)
+        ref = xg.at[ph, 0:rows] if ph < 3 else wof.at[0:rows, batches[ph - 3][0] : batches[ph - 3][2]]
+        remote(ref, ref, ag_send.at[ph], ag_recv.at[ph, slot], mate).wait_recv()
 
     def ag_start(ph):
         ag(ph, 0, xi, ci, H0, x_right).start()
@@ -219,9 +226,9 @@
         ag(ph, 8, x3, ci, H1, mate).start()
         ag(ph, 4, x1, ci, H0, x_left).wait_recv()
         ag(ph, 11, x1, ci, H0, mate).start()
-        ag(ph, 6, xi, oc, every, mate).wait_recv()
-        for i, xx, cols in ((7, x3, H0), (10, x1, H1), (8, x3, H1), (11, x1, H0)):
-            ag(ph, i, xx, oc, cols, mate).wait_recv()
+        if ph != 2:
+            from_mate(ph, 6, 1)
+        from_mate(ph, 7, 2)
 
     def ag_far(ph):
         ag(ph, 2, x2, ci, H0, x_right).wait_recv()
@@ -230,8 +237,7 @@
         ag(ph, 12, x2, ci, H1, mate).start()
 
     def ag_end(ph):
-        ag(ph, 9, x2, oc, H0, mate).wait_recv()
-        ag(ph, 12, x2, oc, H1, mate).wait_recv()
+        from_mate(ph, 8, 1)
 
     def ag_sent(ph):
         ref = xg.at[ph, 0 : 7 * T] if ph < 3 else wof.at[0 : 7 * 128, batches[ph - 3][0] : batches[ph - 3][2]]
@@ -245,7 +251,7 @@
             src, dst = pp.at[ph, :, pl.ds(k * W, W)], rp.at[ph, :, pl.ds(k * W, W)]
         else:
             src, dst = st.at[ph, i, :, pl.ds(k * V, V)], rt.at[ph, i, :, pl.ds(k * V, V)]
-        return remote(src, dst, rs_send.at[ph, i // 6], rs_recv.at[ph, k, i], dev)
+        return remote(src, dst, rs_send.at[ph, i // 6], rs_recv.at[ph, k, (0, 2, 2, 1, 2, 2, 3)[i]], dev)
 
     rs_dev = (x_right, x_right, x_right, x_left, x_left, x_left, mate)
     my_rows = pl.ds(mo(ci * 4 * T, 16), 4 * T)
@@ -294,8 +300,8 @@
 
     def rs_d(ph, k):
         lo, hi, to = k * W, k * W + V, pl.ds(k * V, V)
-        for i in (1, 4, 2, 5):
-            rs(ph, k, i, rs_dev[i]).wait_recv()
+        ref = rt.at[ph, 0:4, :, pl.ds(0, V)]
+        remote(ref, ref, rs_send.at[ph, 0], rs_recv.at[ph, k, 2], mate).wait_recv()
         low = part(ph, xi, lo) + rt[ph, 2, :, to].astype(f32) + rt[ph, 4, :, to].astype(f32)
         high = part(ph, xi, hi) + rt[ph, 1, :, to].astype(f32) + rt[ph, 5, :, to].astype(f32)
         for i in range(BLOCKS // 2):
@@ -329,26 +335,44 @@
     def rows_at(cc, xx):
         return pl.ds(mo((cc * 4 + xx) * T, 16), T)
 
-    def expand(ph, j0, j1, chips=None):
-        where = None if chips is None else [rows_at(cc, xx) for xx in chips for cc in (0, 1)]
+    def expand(ph, j0, j1, chips):
+        where = [rows_at(cc, xx) for xx in chips for cc in (0, 1)]
 
         def one(j, _):
             w = gu[:, pl.ds(mo(j * 256, 256), 256)]
             to = pl.ds(mo(j * 128, 128), 128)
-            if where is None:
-                p = dot(xg[ph], w)
-            else:
-                p = dot(jnp.concatenate([xg[ph, r, :] for r in where], axis=0), w)
+            p = dot(jnp.concatenate([xg[ph, r, :] for r in where], axis=0), w)
             gate, up = p[:, 0:128], p[:, 128:256]
             h = (gate / (1.0 + jnp.exp(-gate)) * up).astype(bf16)
-            if where is None:
-                hb[:, to] = h
+            for i, r in enumerate(where):
+                hb[r, to] = h[i * T : i * T + T, :]
+            return 0
+
+        lax.fori_loop(j0, j1, one, 0)
+
+    def accumulate(o1, o2, first=False, last=False):
+        def one(j, _):
+            cols = pl.ds(mo(j * 256, 256), 256)
+            w = jnp.concatenate([gu[rows_of(o1), cols], gu[rows_of(o2), cols]], axis=0)
+            p = dot(jnp.concatenate([xg[0, :, rows_of(o1)], xg[0, :, rows_of(o2)]], axis=1), w)
+            if not first:
+                p = p + acc[:, cols]
+            if last:
+                gate, up = p[:, 0:128], p[:, 128:256]
+                hb[:, pl.ds(mo(j * 128, 128), 128)] = (gate / (1.0 + jnp.exp(-gate)) * up).astype(bf16)
             else:
-                for i, r in enumerate(where):
-                    hb[r, to] = h[i * T : i * T + T, :]
+                acc[:, cols] = p
             return 0
 
-        lax.fori_loop(j0, j1, one, 0)
+        lax.fori_loop(0, F // 128, one, 0)
+
+    def expand_pair(dist):
+        with jax.named_scope(f"pair_{dist}"):
+            gu_done(dist)
+            if dist == H:
+                accumulate(zi, origin(LEFT, H), last=True)
+            else:
+                accumulate(origin(RIGHT, dist), origin(LEFT, dist), first=dist == 1)
 
     def setup_attention():
         t = lax.broadcasted_iota(jnp.int32, (128, 256), 0)
@@ -373,6 +397,13 @@
             wle2[:, lanes] = wle[...].astype(f32)
             bias2[:, lanes] = bias[...]
             qb[own, lanes] = wqk[h].astype(f32).T.astype(bf16)
+        qb[:, 384:512] = jnp.zeros((D, 128), bf16)
+        for i in range(D // 128):
+            qb[i * 128 : i * 128 + 128, 384 : 384 + wls.shape[0]] = (
+                wls[:, i * 128 : i * 128 + 128].astype(f32).T.astype(bf16)
+            )
+        for h in range(2):
+            lanes = slice(h * 64, h * 64 + 64)
             for i in range(8 * T // 128):
                 extra2[i * 128 : i * 128 + 128, lanes] = extra[:, i * 128 : i * 128 + 128].T
 
@@ -383,8 +414,9 @@
         p1 = dot(a, qb[:, 0:256])
         qk[to, :] = p1[:, 0:128].astype(bf16).astype(f32)
         vb[to, :] = p1[:, 128:256].astype(bf16)
-        og[to, :] = dot(a, qb[:, 256:384]).astype(bf16).astype(f32)
-        low = dot_t(a, wls[...]).astype(bf16)
+        p2 = dot(a, qb[:, 256:512])
+        og[to, :] = p2[:, 0:128].astype(bf16).astype(f32)
+        low = p2[:, 128 : 128 + wls.shape[0]].astype(bf16)
         pre = dot(low, wle2[...].astype(bf16)) + bias2[...]
         decay = (jnp.minimum(pre, 0.0) - jnp.log1p(jnp.exp(-jnp.abs(pre)))) / STEEP
         lg[to, :] = decay + extra2[pl.ds(mo(b * SEQ, 16), SEQ), :]
@@ -473,8 +505,8 @@
     def landed(k):
         advance(OFFSETS[1] + 2 * k + 3)
         with scope("dn_done"):
-            for dist, d in order[max(1, 4 * k) : 4 * k + 4]:
-                dn_done(dist, d)
+            dn_done(2 * k + 1)
+            dn_done(2 * k + 2)
 
     def more(count):
         advance(at_tick[0] + count - 1)
@@ -495,36 +527,32 @@
         ag_far(0)
     advance(4)
     ag_end(0)
-    advance(NEAR + 2)
+    advance(5)
+    for dist in (1, 2, 3):
+        expand_pair(dist)
+    advance(6)
+    expand_pair(4)
+    advance(7)
     with scope("ob_near"):
         ob_done(0)
         ag_start(3)
-    advance(NEAR + 3)
+    expand_pair(5)
+    advance(8)
     with scope("ob_mid"):
         ag_mid(3)
-    advance(OFFSETS[0] + H + 1)
-    with scope("ob_far"):
-        ag_near(3)
-        ag_far(3)
-    with scope("gu_done"):
-        z_done(0)
+    expand_pair(6)
+    expand_pair(7)
+    advance(9)
+    expand_pair(8)
 
     def other(what, k):
         if what == "w":
             landed(k)
         elif what == "t":
             more(1)
-        elif what == "g":
-            if k == 0:
-                ob_done(1)
-                ag_start(4)
-            elif k == 1:
-                ag_mid(4)
-            else:
-                ag_near(4)
-                ag_far(4)
         else:
-            expand(0, 3 * k, 3 + 2 * k)
+            ag_near(3)
+            ag_far(3)
 
     run(0, hb, dn, FIRST, other)
     with scope("norm"):
@@ -533,14 +561,16 @@
     z_sent(0)
     z_sent(1)
     ag_sent(0)
-    more(1)
+    more(2)
     with scope("ag1_mid"):
         ag_mid(1)
     advance(last_tick)
     with scope("ag1_near"):
         ag_near(1)
     with scope("qb_done"):
-        z_done(2)
+        qb_done()
+        ob_done(1)
+        ag_start(4)
     seq = lax.div(xi, 2)
     pair = xi + 1 - 2 * lax.rem(xi, 2)
     away = 2 * (1 - seq)
@@ -555,10 +585,15 @@
         ag_end(1)
     with scope("project"):
         project(1 - seq)
+    with scope("ob2_mid"):
+        ag_mid(4)
     with scope("attend"):
         attend(1 - seq)
         hand_out(1, ((away, 0), (away, 1), (away + 1, 0), (away + 1, 1)))
     ga[:, my_cols] = gt[own_rows, :]
+    with scope("ob2_far"):
+        ag_near(4)
+        ag_far(4)
     with scope("ob_end"):
         ag_end(3)
         ag_end(4)
@@ -577,11 +612,14 @@
         ag_sent(i)
     handed(0, 3).wait_send()
     handed(1, 4).wait_send()
+    with scope("expand_own"):
+        from_mate(2, 6, 1)
+        expand(2, 0, 5, (xi,))
     with scope("ag2_mid"):
         ag_mid(2)
     with scope("ag2_near"):
         ag_near(2)
-    near = (xi, x1, x3)
+    near = (x1, x3)
     with scope("expand_near"):
         expand(2, 0, 3, near)
     with scope("ag2_far"):
@@ -620,10 +658,11 @@
             scratch_shapes=[
                 pltpu.VMEM((D, 2 * F), bf16),
                 pltpu.VMEM((F, D), bf16),
-                pltpu.VMEM((D, 384), bf16),
+                pltpu.VMEM((D, 512), bf16),
                 pltpu.VMEM((8 * 128, D), bf16),
                 pltpu.VMEM((T, 8 * 128), bf16),
                 pltpu.VMEM((3, N8, D), bf16),
+                pltpu.VMEM((N8, 2 * F), f32),
                 pltpu.VMEM((N8, F), bf16),
                 pltpu.VMEM((2, N8 // 2, D), bf16),
                 pltpu.VMEM((2, N8 // 2, D), bf16),
@@ -646,18 +685,19 @@
                 pltpu.VMEM((1, bias.shape[0]), f32),
                 pltpu.VMEM((extra.shape[1], extra.shape[0]), f32),
                 pltpu.VMEM((1, gain.shape[0]), f32),
-                dma((4, 2, 2, n // 2)),
-                dma((4,)),
-                dma((n // 2, 2)),
+                dma((3, 2, 2, n // 2)),
+                dma((n // 2,)),
+                dma((n // 2,)),
+                dma((1,)),
                 dma((2,)),
                 dma((4, 3)),
-                dma((5, 13)),
+                dma((5, 9)),
                 dma((5,)),
-                dma((2, CHUNKS, 7)),
+                dma((2, CHUNKS, 4)),
                 dma((2, 2)),
                 dma((2,)),
                 dma((2,)),
-                dma((2 * F // 128 + 12,)),
+                dma((13,)),
             ],
             compiler_params=pltpu.CompilerParams(
                 collective_id=0, has_side_effects=True, vmem_limit_bytes=60 * 1024 * 1024

time: 171 us -> 164 us (0.959)
  Pallas kernels: 169 us -> 162 us
    pallas_call x1, Pallas kernels: 169 us -> 162 us  [per_device(): pl.pallas_call(functools.partial(kernel, n), out_shape=jax.ShapeDtypeStru...]
where the time goes in v3:
time: 164 us
  Pallas kernels  162 us (99%)
  local copies, waits for them, and re-layouts  1.72 us (1%)
    pallas_call x1, Pallas kernels, per_device(): pl.pallas_call(functools.partial(kernel, n), out_shape=jax.ShapeDtypeStru...  162 us

profile of v3, /device:TPU:33, one launch (start us, length us, event | category | flops | bytes accessed | tf_op | source)
XLA Modules:
  0.0 163.8 jit_solution(15482511491061693916)
XLA Ops:
  0.0 162.1 %shard_map.136 = bf16[80,2048]{1,0:T(8,128)(2,1)} custom-call(bf16[80,2048]{1,0:T(8,128)(2,1)} %x_in.1, bf16[128,640]{1,0:T(8,128)(2,1)} %wsw.1, bf16[128,640]{1,0:T(8,128)(2,1)} %wex.1, bf16[640,128]{1,0:T(8,128)(2,1)} %wct.1, bf16[64,128]{1,0:T(8,128)(2,1)} %bitcast.8, bf16[64,128]{1,0:T(8,128)(2,1)} %bitcast.9, bf16[128,128]{1,0:T(8,128)(2,1)} %wv.1, ...), custom_call_target="tpu_custom_call" | custom-call | tf_op jit(solution)/shard_map/pallas_call | solution.py:653
  162.1 1.7 %copy.16 = bf16[80,2048]{1,0:T(8,128)(2,1)} copy(bf16[80,2048]{1,0:T(8,128)(2,1)} %shard_map.136) | data formatting | bytes 655360

commit v4 on v3

--- a/solution.py
+++ b/solution.py
@@ -16,10 +16,11 @@
 STEEP = 16.0
 EPS = 1e-06
 CHUNKS = 4
-OFFSETS = (0, 3, 9, 0)
+OFFSETS = (0, 2, 8, 0)
+PAUSE, RESUME = 6, 13
 NEAR = 5
 FIRST = (
-    "t0 w0 o0 m0", "w1 o1 m1 t0", "b0 b1 w2 o2", "m2 t0 b2 c0", "c1 w3 o3 m3", "b3 c2 t0 g2",
+    "t0 w0 o0 m0", "w1 o1 m1 b0", "t0 b1 w2 o2", "m2 b2 w3 o3", "t0 m3 c0 c1", "b3 c2 g2 t0",
     "c3 d0 d1 t0", "d2 d3",
 )
 STEPS = ("o0 o1 m0 b0", "o2 m1 b1 o3", "m2 b2 m3 c0", "b3 c1 c2 c3", "d0 d1 d2 d3")
@@ -111,10 +112,10 @@
         return gu.at[rows_of(o), pl.ds(mo(par * 896, 128), 384) if ch == A else pl.ds(384, 512)]
 
     def dn_at(o, ch):
-        return dn.at[pl.ds(mo(par * 432, 16), 208) if ch == A else pl.ds(208, 224), rows_of(o)]
+        return dn.at[pl.ds(mo(par * 416, 16), 224) if ch == A else pl.ds(224, 192), rows_of(o)]
 
     def qb_at(o, ch):
-        return qb.at[rows_of(o), pl.ds(mo(par * 256, 128), 128) if ch == A else pl.ds(128, 128)]
+        return qb.at[pl.ds(mo(o * K + par * (K // 2), K // 2), K // 2), 0:384]
 
     def ob_at(slot, ch):
         rows = mo(ti * 128 + par * 80, 16) if ch == A else mo(ti * 128 + 48, 16)
@@ -127,8 +128,8 @@
     R = (n - 1) * K
     whole = (
         (gu.at[0:R, 0:384], gu.at[0:R, 384:896]),
-        (dn.at[0:208, 0:R], dn.at[208:432, 0:R]),
-        (qb.at[0:R, 0:128], qb.at[0:R, 128:256]),
+        (dn.at[0:224, 0:R], dn.at[224:416, 0:R]),
+        (qb.at[0 : R // 2, 0:384], None),
         (wof.at[0:48, 0:R], wof.at[48:80, 0:R]),
     )
 
@@ -148,11 +149,15 @@
     def tick(t):
         for m in range(4):
             s = t - OFFSETS[m]
+            if m == 3 and t > PAUSE:
+                s = t - RESUME + PAUSE + 1
+                if s <= PAUSE:
+                    continue
             if s < 1 or s > H + 1:
                 continue
             for ch, d in ((A, RIGHT), (A, LEFT), (B, RIGHT), (B, LEFT)):
                 last = steps_of(ch, d)
-                if s - 1 > last:
+                if s - 1 > last or (m == 2 and ch == B):
                     continue
                 o = origin(d, s - 1)
                 if s > 1:
@@ -173,7 +178,7 @@
         remote(ref, ref, z_send.at[0, 2], c_gu.at[dist - 1], y_dev).wait_recv()
 
     def dn_done(dist):
-        ref = dn.at[0:208, 0 : (2 if dist < H else 1) * K]
+        ref = dn.at[0:224, 0 : (2 if dist < H else 1) * K]
         remote(ref, ref, z_send.at[1, 2], c_dn.at[dist - 1], y_dev).wait_recv()
 
     def ob_done(batch):
@@ -183,6 +188,8 @@
     def z_sent(m):
         for ch, i in ((A, A), (B, B), (A, 2)):
             w = whole[m][ch]
+            if w is None:
+                continue
             remote(w, w, z_send.at[m, i], c_qb.at[0], y_dev).wait_send()
 
     H0, H1 = pl.ds(0, D // 2), pl.ds(D // 2, D // 2)
@@ -226,6 +233,10 @@
         ag(ph, 8, x3, ci, H1, mate).start()
         ag(ph, 4, x1, ci, H0, x_left).wait_recv()
         ag(ph, 11, x1, ci, H0, mate).start()
+        if ph < 3:
+            ag_near_mate(ph)
+
+    def ag_near_mate(ph):
         if ph != 2:
             from_mate(ph, 6, 1)
         from_mate(ph, 7, 2)
@@ -485,8 +496,8 @@
         ref = gt.at[0 : count * T]
         return remote(ref, ref, aa_send.at[i], aa_recv.at[i], mate)
 
-    def emit():
-        for slot in range(0, n, 2):
+    def emit(slots):
+        for slot in slots:
             p = dot(ga[...], wof[:, slot * K : slot * K + 2 * K])
             for i in range(2):
                 o = lax.rem(zi + n + slot + i - NEAR, n)
@@ -568,9 +579,9 @@
     with scope("ag1_near"):
         ag_near(1)
     with scope("qb_done"):
-        qb_done()
         ob_done(1)
         ag_start(4)
+        qb_done()
     seq = lax.div(xi, 2)
     pair = xi + 1 - 2 * lax.rem(xi, 2)
     away = 2 * (1 - seq)
@@ -594,14 +605,18 @@
     with scope("ob2_far"):
         ag_near(4)
         ag_far(4)
-    with scope("ob_end"):
+        ag_near_mate(3)
         ag_end(3)
-        ag_end(4)
     with scope("handed"):
         handed(0, 3).wait_recv()
         handed(1, 4).wait_recv()
     with scope("emit"):
-        emit()
+        emit(range(0, 2 * NEAR, 2))
+    with scope("ob_end"):
+        ag_near_mate(4)
+        ag_end(4)
+    with scope("emit"):
+        emit(range(2 * NEAR, n, 2))
     with scope("norm"):
         xg[2, own_rows, :] = post_norm(1, 1.0)
     ag_start(2)

time: 164 us -> 161 us (0.982)
  Pallas kernels: 162 us -> 159 us
    pallas_call x1, Pallas kernels: 162 us -> 159 us  [per_device(): pl.pallas_call(functools.partial(kernel, n), out_shape=jax.ShapeDtypeStru...]
where the time goes in v4:
time: 161 us
  Pallas kernels  159 us (99%)
  local copies, waits for them, and re-layouts  1.72 us (1%)
    pallas_call x1, Pallas kernels, per_device(): pl.pallas_call(functools.partial(kernel, n), out_shape=jax.ShapeDtypeStru...  159 us

profile of v4, /device:TPU:33, one launch (start us, length us, event | category | flops | bytes accessed | tf_op | source)
XLA Modules:
  0.0 161.0 jit_solution(2355503441785209871)
XLA Ops:
  0.0 159.3 %shard_map.136 = bf16[80,2048]{1,0:T(8,128)(2,1)} custom-call(bf16[80,2048]{1,0:T(8,128)(2,1)} %x_in.1, bf16[128,640]{1,0:T(8,128)(2,1)} %wsw.1, bf16[128,640]{1,0:T(8,128)(2,1)} %wex.1, bf16[640,128]{1,0:T(8,128)(2,1)} %wct.1, bf16[64,128]{1,0:T(8,128)(2,1)} %bitcast.8, bf16[64,128]{1,0:T(8,128)(2,1)} %bitcast.9, bf16[128,128]{1,0:T(8,128)(2,1)} %wv.1, ...), custom_call_target="tpu_custom_call" | custom-call | tf_op jit(solution)/shard_map/pallas_call | solution.py:668
  159.3 1.7 %copy.16 = bf16[80,2048]{1,0:T(8,128)(2,1)} copy(bf16[80,2048]{1,0:T(8,128)(2,1)} %shard_map.136) | data formatting | bytes 655360

commit v5 on v4

--- a/solution.py
+++ b/solution.py
@@ -118,8 +118,7 @@
         return qb.at[pl.ds(mo(o * K + par * (K // 2), K // 2), K // 2), 0:384]
 
     def ob_at(slot, ch):
-        rows = mo(ti * 128 + par * 80, 16) if ch == A else mo(ti * 128 + 48, 16)
-        return wof.at[pl.ds(rows, 48 if ch == A else 32), pl.ds(slot * K, K)]
+        return wof.at[pl.ds(mo(ti * 128 + par * 64, 64), 64), pl.ds(slot * K, K)]
 
     def ob_slot(d, dist):
         return (NEAR - dist) % n if d == RIGHT else (NEAR + dist) % n
@@ -130,7 +129,7 @@
         (gu.at[0:R, 0:384], gu.at[0:R, 384:896]),
         (dn.at[0:224, 0:R], dn.at[224:416, 0:R]),
         (qb.at[0 : R // 2, 0:384], None),
-        (wof.at[0:48, 0:R], wof.at[48:80, 0:R]),
+        (wof.at[0:64, 0:R], None),
     )
 
     def steps_of(ch, d):
@@ -144,7 +143,7 @@
             src, dst = ob_at(ob_slot(d, s - 1), ch), ob_at(ob_slot(d, s), ch)
         else:
             src = dst = at[m](o, ch)
-        return remote(src, dst, z_send.at[m, ch], z_recv.at[(0, 1, 0, 2)[m], d, ch, s - 1], z_dev[d])
+        return remote(src, dst, z_send.at[m, ch], z_recv.at[(0, 2, 0, 4)[m] + ch, d, (s - 1) % 4], z_dev[d])
 
     def tick(t):
         for m in range(4):
@@ -157,7 +156,7 @@
                 continue
             for ch, d in ((A, RIGHT), (A, LEFT), (B, RIGHT), (B, LEFT)):
                 last = steps_of(ch, d)
-                if s - 1 > last or (m == 2 and ch == B):
+                if s - 1 > last or (m >= 2 and ch == B):
                     continue
                 o = origin(d, s - 1)
                 if s > 1:
@@ -182,7 +181,7 @@
         remote(ref, ref, z_send.at[1, 2], c_dn.at[dist - 1], y_dev).wait_recv()
 
     def ob_done(batch):
-        ref = wof.at[0:48, 0 : (2 * NEAR if batch == 0 else n - 1 - 2 * NEAR) * K]
+        ref = wof.at[0:64, 0 : (2 * NEAR if batch == 0 else n - 1 - 2 * NEAR) * K]
         remote(ref, ref, z_send.at[3, 2], c_ob.at[batch], y_dev).wait_recv()
 
     def z_sent(m):
@@ -667,7 +666,7 @@
         dma = pltpu.SemaphoreType.DMA
         return pl.pallas_call(
             functools.partial(kernel, n),
-            out_shape=jax.ShapeDtypeStruct((T, D), bf16),
+            out_shape=pltpu.VMEM((T, D), bf16),
             in_specs=[anywhere] * 14,
             out_specs=vmem,
             scratch_shapes=[
@@ -700,7 +699,7 @@
                 pltpu.VMEM((1, bias.shape[0]), f32),
                 pltpu.VMEM((extra.shape[1], extra.shape[0]), f32),
                 pltpu.VMEM((1, gain.shape[0]), f32),
-                dma((3, 2, 2, n // 2)),
+                dma((5, 2, 4)),
                 dma((n // 2,)),
                 dma((n // 2,)),
                 dma((1,)),

time: 161 us -> 159 us (0.988)
  no operation moved by 1% of the time
where the time goes in v5:
time: 159 us; the launch traced here: 158 us
  Pallas kernels  158 us (99%)
    pallas_call x1, Pallas kernels, per_device(): pl.pallas_call(functools.partial(kernel, n), out_shape=pltpu.VMEM((T, D),...  158 us

profile of v5, /device:TPU:33, one launch (start us, length us, event | category | flops | bytes accessed | tf_op | source)
XLA Modules:
  0.0 158.5 jit_solution(17100743098432745092)
XLA Ops:
  0.0 157.8 %shard_map.136 = bf16[80,2048]{1,0:T(8,128)(2,1)S(1)} custom-call(bf16[80,2048]{1,0:T(8,128)(2,1)} %x_in.1, bf16[128,640]{1,0:T(8,128)(2,1)} %wsw.1, bf16[128,640]{1,0:T(8,128)(2,1)} %wex.1, bf16[640,128]{1,0:T(8,128)(2,1)} %wct.1, bf16[64,128]{1,0:T(8,128)(2,1)} %bitcast.8, bf16[64,128]{1,0:T(8,128)(2,1)} %bitcast.9, bf16[128,128]{1,0:T(8,128)(2,1)} %wv.1, ...), custom_call_target="tpu_custom_call" | custom-call | tf_op jit(solution)/shard_map/pallas_call | solution.py:667
  157.8 0.7 copy.16
